TPU v7x, 32 devices: a whole 2x2x4 slice. The times are simulated.
32 devices in a mesh: ep: 8 (over z, x), tp: 4 (over y, core).
Axes of the slice: x: 2, y: 2, z: 4, core: 2. Of those that a mesh axis runs over, the one named last changes fastest.
Arguments:
- mixer_input: bfloat16 [2048, 2048], P('ep'), may hold values from -6 to 6
- mixer_gain: float32 [2048], replicated, may hold values from 0.1 to 8
- query_one: bfloat16 [2048, 512], P(None, 'tp'), may hold values from -0.1875 to 0.1875
- query_two: bfloat16 [2048, 512], P(None, 'tp'), may hold values from -0.1875 to 0.1875
- key_one: bfloat16 [2048, 256], P(None, 'tp'), may hold values from -0.1875 to 0.1875
- key_two: bfloat16 [2048, 256], P(None, 'tp'), may hold values from -0.1875 to 0.1875
- value_weight: bfloat16 [2048, 512], P(None, 'tp'), may hold values from -0.125 to 0.125
- lambdas: float32 [8], P('tp'), may hold values from 0.3 to 0.8
- head_gain: float32 [128], replicated, may hold values from 0.1 to 1.9
- output_weight: bfloat16 [1024, 2048], P('tp'), may hold values from -0.1875 to 0.1875
- expert_input: bfloat16 [4096, 2048], P(('ep', 'tp')), may hold values from -6 to 6
- expert_gain: float32 [2048], replicated, may hold values from 0.1 to 1.9
- routes: int32 [4096, 2], P(('ep', 'tp')), may hold values from 0 to 7, all different within a row; in each aligned block of 128 rows (0 to 127, 128 to 255, ...) at most 40 rows name the same one
- route_weight: float32 [4096, 2], P(('ep', 'tp')), may hold values from 0.2 to 1
- expert_gate: bfloat16 [8, 2048, 1024], P('ep', None, 'tp'), may hold values from -0.125 to 0.125
- expert_up: bfloat16 [8, 2048, 1024], P('ep', None, 'tp'), may hold values from -0.125 to 0.125
- expert_down: bfloat16 [8, 1024, 2048], P('ep', 'tp'), may hold values from -0.1875 to 0.1875
- shared_gate: bfloat16 [2048, 512], P(None, 'tp'), may hold values from -0.125 to 0.125
- shared_up: bfloat16 [2048, 512], P(None, 'tp'), may hold values from -0.125 to 0.125
- shared_down: bfloat16 [512, 2048], P('tp'), may hold values from -0.25 to 0.25
Outputs:
- mixer_output: bfloat16 [2048, 2048], P(('ep', 'tp'))
- expert_output: bfloat16 [4096, 2048], P(('ep', 'tp'))
Inputs may be any that keep to these rules, and one draw needn't show every extreme that they name: `routes`: each row names 2 different experts; in the rows of one device no expert is named by more than 40 rows, and some device names some expert exactly 40 times.
All inputs are finite; a program needn't handle non-finite values.
Results may differ from a plain program's by a relative error of at most 0.014.
The roundings to bfloat16 on the way count: a program that leaves them out, or rounds other values in their place, can miss the bound.
Values may be sent and summed in bfloat16 or wider, within the bound.
A program may use at most 128 MiB of HBM per device.

v0:
```python
import functools
import math

import jax
import jax.numpy as jnp
from jax import lax
from jax.experimental import pallas as pl
from jax.experimental.pallas import tpu as pltpu
from jax.sharding import PartitionSpec as P

HEAD = 64


EPS = 1e-06
NEG = -1e30


def normalize(activations, scaling):
    values = activations.astype(jnp.float32)
    factor = lax.rsqrt(jnp.mean(values * values, axis=-1, keepdims=True) + EPS)
    return (values * factor * scaling).astype(jnp.bfloat16)


def attention_kernel(
    shape, rank_ref, lambdas_ref, queries_ref, keys_ref, gain_ref, out_ref, maxima, totals, weighted
):
    rows, chunk, local_kv, group, value_dim = shape
    rank = rank_ref[0]
    maxima[...] = jnp.full(maxima.shape, NEG, jnp.float32)
    totals[...] = jnp.zeros(totals.shape, jnp.float32)
    weighted[...] = jnp.zeros(weighted.shape, jnp.float32)
    heads = local_kv * group
    key_cols = local_kv * HEAD
    chunks = rows // chunk
    scale = HEAD**-0.5 * math.log2(math.e)

    def block(index, masked):
        start = pl.multiple_of(index * rows, rows)
        for kv in range(local_kv):
            value_start = 2 * key_cols + kv * value_dim
            for part in range(chunks):
                span = (part + 1) * chunk if masked else rows
                values = keys_ref[pl.ds(start, span), value_start : value_start + value_dim]
                for which in range(2):
                    first = which * key_cols + kv * HEAD
                    keys = keys_ref[pl.ds(start, span), first : first + HEAD]
                    for g in range(group):
                        head = kv * group + g
                        col = (which * heads + head) * HEAD
                        queries = queries_ref[part * chunk : (part + 1) * chunk, col : col + HEAD]
                        scores = lax.dot_general(
                            queries,
                            keys,
                            (((1,), (1,)), ((), ())),
                            preferred_element_type=jnp.float32,
                        )
                        if masked:
                            row = part * chunk + lax.broadcasted_iota(jnp.int32, scores.shape, 0)
                            col_pos = lax.broadcasted_iota(jnp.int32, scores.shape, 1)
                            scores = jnp.where(col_pos <= row, scores, NEG)
                        slot = (which * heads + head) * chunks + part
                        earlier = maxima[slot]
                        latest = jnp.maximum(earlier, jnp.max(scores, axis=1, keepdims=True))
                        shrink = jnp.exp2((earlier - latest) * scale)
                        weights = jnp.exp2((scores - latest[:, :1]) * scale)
                        totals[slot] = totals[slot] * shrink + jnp.sum(
                            weights, axis=1, keepdims=True
                        )
                        weighted[slot] = weighted[slot] * shrink[:, :1] + jnp.dot(
                            weights.astype(jnp.bfloat16),
                            values,
                            preferred_element_type=jnp.float32,
                        )
                        maxima[slot] = latest

    def earlier_block(index, carry):
        block(index, False)
        return carry

    lax.fori_loop(0, rank, earlier_block, 0)
    block(rank, True)
    for head in range(heads):
        for part in range(chunks):
            one = head * chunks + part
            two = (heads + head) * chunks + part
            combined = (
                weighted[one] / totals[one][:, :1]
                - lambdas_ref[head] * (weighted[two] / totals[two][:, :1])
            )
            factor = lax.rsqrt(jnp.mean(combined * combined, axis=1, keepdims=True) + EPS)
            out_ref[
                part * chunk : (part + 1) * chunk, head * value_dim : (head + 1) * value_dim
            ] = (combined * factor * gain_ref[...]).astype(jnp.bfloat16)


def attention(queries, keys, rank, lambdas, head_gain, local_kv, group):
    rows = queries.shape[0]
    value_dim = head_gain.shape[0]
    heads = local_kv * group
    chunk = min(128, rows)
    slots = 2 * heads * (rows // chunk)
    vmem = pl.BlockSpec(memory_space=pltpu.VMEM)
    smem = pl.BlockSpec(memory_space=pltpu.SMEM)
    scores = heads * 2 * rows * keys.shape[0]
    return pl.pallas_call(
        functools.partial(attention_kernel, (rows, chunk, local_kv, group, value_dim)),
        out_shape=jax.ShapeDtypeStruct((rows, heads * value_dim), jnp.bfloat16),
        in_specs=[smem, smem, vmem, vmem, vmem],
        out_specs=vmem,
        scratch_shapes=[
            pltpu.VMEM((slots, chunk, 128), jnp.float32),
            pltpu.VMEM((slots, chunk, 128), jnp.float32),
            pltpu.VMEM((slots, chunk, value_dim), jnp.float32),
        ],
        compiler_params=pltpu.CompilerParams(vmem_limit_bytes=48 * 1024 * 1024),
        cost_estimate=pl.CostEstimate(
            flops=8 * scores * HEAD, bytes_accessed=keys.size * 2, transcendentals=scores
        ),
        name="attention",
    )(rank.reshape(1), lambdas, queries, keys, head_gain.reshape(1, value_dim))


def swap(rows, axis, size, distance):
    return lax.ppermute(rows, axis, [(i, i ^ distance) for i in range(size)])


def gather_near(block, axis, size, ahead=None):
    places = {0: block}
    distance = size // 2
    while distance:
        for place in sorted(places):
            moved = swap(places[place], axis, size, distance)
            if ahead is not None:
                moved, ahead = lax.optimization_barrier((moved, ahead))
            places[place ^ distance] = moved
        ahead = None
        distance //= 2
    return [places[place] for place in range(size)]


def scatter_near(partials, axis, size):
    sums = dict(enumerate(partials))
    distance = 1
    while distance < size:
        kept = [place for place in sorted(sums) if not place & distance]
        moved = {
            place: swap(sums[place ^ distance].astype(jnp.bfloat16), axis, size, distance)
            for place in kept
        }
        sums = {
            place: sums[place].astype(jnp.float32) + moved[place].astype(jnp.float32)
            for place in kept
        }
        distance *= 2
    return sums[0]


def body(
    mixer_input,
    mixer_gain,
    query_one,
    query_two,
    key_one,
    key_two,
    value_weight,
    lambdas,
    head_gain,
    output_weight,
    expert_input,
    expert_gain,
    routes,
    route_weight,
    expert_gate,
    expert_up,
    expert_down,
    shared_gate,
    shared_up,
    shared_down,
):
    ep_size = lax.axis_size("ep")
    tp_size = lax.axis_size("tp")
    ep_rank = lax.axis_index("ep")
    mixer_rows = mixer_input.shape[0]
    model_width = mixer_input.shape[1]
    query_cols = query_one.shape[1]
    key_cols = key_one.shape[1]
    value_dim = head_gain.shape[0]
    local_kv = key_cols // HEAD
    local_heads = query_cols // HEAD
    group_size = local_heads // local_kv
    normed = normalize(mixer_input, mixer_gain)

    def project(weights):
        return jnp.concatenate(
            [
                jnp.dot(normed, weight, preferred_element_type=jnp.float32).astype(jnp.bfloat16)
                for weight in weights
            ],
            axis=1,
        )

    key_values = project([key_one, key_two, value_weight])
    query_part = project([query_one, query_two])
    arrived = lax.all_gather(key_values, "ep", axis=0, tiled=True)
    head_rows = attention(
        query_part, arrived, ep_rank, lambdas, head_gain, local_kv, group_size
    )
    tp_rank = lax.axis_index("tp")
    own_rows = mixer_rows // tp_size

    def mixer_place(place):
        rows = lax.dynamic_slice_in_dim(head_rows, (tp_rank ^ place) * own_rows, own_rows, 0)
        return jnp.dot(rows, output_weight, preferred_element_type=jnp.float32).astype(
            jnp.bfloat16
        )

    mixer_sum = scatter_near(
        [mixer_place(place) for place in range(tp_size)], "tp", tp_size
    ).astype(jnp.bfloat16)

    token_rows = expert_input.shape[0]
    normed_experts = normalize(expert_input, expert_gain)
    experts_local = expert_gate.shape[0]
    expert_count = experts_local * ep_size
    top_count = routes.shape[1]
    capacity = max(2, 5 * token_rows * top_count // (4 * expert_count))
    slot_count = expert_count * capacity
    flat_routes = routes.reshape(-1)
    onehot = (flat_routes[:, None] == jnp.arange(expert_count, dtype=jnp.int32)[None, :]).astype(
        jnp.int32
    )
    slot_place = jnp.sum((jnp.cumsum(onehot, axis=0) - onehot) * onehot, axis=1)
    slot_ids = (flat_routes * capacity + slot_place).reshape(token_rows, top_count)
    slot_match = jnp.arange(slot_count, dtype=jnp.int32)[:, None, None] == slot_ids[None, :, :]
    select = jnp.any(slot_match, axis=2).astype(jnp.bfloat16)
    outgoing = jnp.dot(select, normed_experts, preferred_element_type=jnp.float32).astype(
        jnp.bfloat16
    )
    pair_rows = experts_local * capacity
    outgoing = outgoing.reshape(ep_size, pair_rows, model_width)
    outgoing, key_values = lax.optimization_barrier((outgoing, key_values))
    received = lax.all_to_all(outgoing, "ep", split_axis=0, concat_axis=0, tiled=True)
    received = received.reshape(ep_size, experts_local, capacity, model_width)
    if experts_local == 1:
        received = received.reshape(ep_size * capacity, model_width)

    def shared_expert(rows):
        gated = jnp.dot(rows, shared_gate, preferred_element_type=jnp.float32)
        lifted = jnp.dot(rows, shared_up, preferred_element_type=jnp.float32)
        hidden = (jax.nn.silu(gated) * lifted).astype(jnp.bfloat16)
        return jnp.dot(hidden, shared_down, preferred_element_type=jnp.float32).astype(
            jnp.bfloat16
        )

    def routed_expert(rows):
        if experts_local == 1:
            gated = jnp.dot(rows, expert_gate[0], preferred_element_type=jnp.float32)
            lifted = jnp.dot(rows, expert_up[0], preferred_element_type=jnp.float32)
            hidden = (jax.nn.silu(gated) * lifted).astype(jnp.bfloat16)
            return jnp.dot(hidden, expert_down[0], preferred_element_type=jnp.float32).astype(
                jnp.bfloat16
            )
        gated = jnp.einsum("secd,edf->secf", rows, expert_gate, preferred_element_type=jnp.float32)
        lifted = jnp.einsum("secd,edf->secf", rows, expert_up, preferred_element_type=jnp.float32)
        hidden = (jax.nn.silu(gated) * lifted).astype(jnp.bfloat16)
        return jnp.einsum(
            "secf,efd->secd", hidden, expert_down, preferred_element_type=jnp.float32
        ).astype(jnp.bfloat16)

    shared_places = gather_near(normed_experts, "tp", tp_size)
    routed_places = gather_near(received, "tp", tp_size, head_rows)
    shared_result = scatter_near([shared_expert(rows) for rows in shared_places], "tp", tp_size)
    routed_result = scatter_near(
        [routed_expert(rows) for rows in routed_places], "tp", tp_size
    ).astype(jnp.bfloat16)
    returned = lax.all_to_all(
        routed_result.reshape(ep_size, pair_rows, model_width),
        "ep",
        split_axis=0,
        concat_axis=0,
        tiled=True,
    )
    returned = returned.reshape(slot_count, model_width)
    spread = jnp.sum(
        jnp.where(
            jnp.arange(slot_count, dtype=jnp.int32)[None, None, :] == slot_ids[:, :, None],
            route_weight[:, :, None],
            0.0,
        ),
        axis=1,
    )
    upper = lax.reduce_precision(spread, 8, 7)
    lower = lax.reduce_precision(spread - upper, 8, 7)
    routed_total = jnp.dot(
        upper.astype(jnp.bfloat16), returned, preferred_element_type=jnp.float32
    ) + jnp.dot(lower.astype(jnp.bfloat16), returned, preferred_element_type=jnp.float32)
    expert_output = (routed_total + shared_result).astype(jnp.bfloat16)
    return (mixer_sum, expert_output)


def solution(mesh):
    in_specs = (
        P("ep", None),
        P(),
        P(None, "tp"),
        P(None, "tp"),
        P(None, "tp"),
        P(None, "tp"),
        P(None, "tp"),
        P("tp"),
        P(),
        P("tp", None),
        P(("ep", "tp"), None),
        P(),
        P(("ep", "tp"), None),
        P(("ep", "tp"), None),
        P("ep", None, "tp"),
        P("ep", None, "tp"),
        P("ep", "tp", None),
        P(None, "tp"),
        P(None, "tp"),
        P("tp", None),
    )
    out_specs = (P(("ep", "tp"), None), P(("ep", "tp"), None))
    return jax.shard_map(body, mesh=mesh, in_specs=in_specs, out_specs=out_specs, check_vma=False)
```

profile of v0, /device:TPU:31, one launch (start us, length us, event | category | flops | bytes accessed | tf_op | source)
XLA Modules:
  0.0 206.6 jit_solution(6992863228179343315)
XLA Ops:
  7.2 0.9 copy.56
  8.1 0.1 eq.56
  8.2 0.1 eq.52
  8.3 1.5 fusion.8
  9.9 1.9 convolution_convert_fusion.17
  11.9 0.5 convolution_convert_fusion.16
  12.6 1.6 convolution_convert_fusion.13
  14.2 0.6 reduce-window.6
  14.8 0.2 slice_reduce_fusion
  15.2 0.1 reduce_sum.40
  15.4 0.2 fusion.13
  15.7 0.2 fusion.15
  15.8 1.6 convolution_convert_fusion
  17.4 0.8 pad_maximum_fusion.1
  18.2 5.4 %all-to-all-start = ((bf16[8,40,2048]{2,1,0:T(8,128)(2,1)}), bf16[8,40,2048]{2,1,0:T(8,128)(2,1)}, u32[]{:S(2)}, u32[]{:S(2)}) async-start(bf16[8,40,2048]{2,1,0:T(8,128)(2,1)} %bitcast.100), calls=%async_computation | async-start | bytes 2621440 | tf_op jit(solution)/shard_map/all_to_all | solution.py:242
  23.6 0.7 all-gather.2.cloned.1.call-update
  24.3 33.4 %all-to-all-done = bf16[8,40,2048]{2,1,0:T(8,128)(2,1)} async-done(((bf16[8,40,2048]{2,1,0:T(8,128)(2,1)}), bf16[8,40,2048]{2,1,0:T(8,128)(2,1)}, u32[]{:S(2)}, u32[]{:S(2)}) %all-to-all-start) | async-done | bytes 1310752 | tf_op jit(solution)/shard_map/all_to_all | solution.py:242
  57.7 0.2 collective-permute-start.5
  57.9 1.5 convolution_convert_fusion.14
  59.5 1.6 convolution_convert_fusion.15
  61.1 12.8 %all-gather.2.cloned.1.call-done.keys_ref = bf16[2048,256]{1,0:T(8,128)(2,1)} async-done(((bf16[256,256]{1,0:T(8,128)(2,1)}), bf16[2048,256]{1,0:T(8,128)(2,1)}) %all-gather.2.cloned.1.call-update) | async-done | bytes 1048592 | tf_op jit(solution)/shard_map/all_gather | solution.py:204
  73.9 1.2 copy-done.1
  75.1 18.6 %attention.1 = bf16[256,256]{1,0:T(8,128)(2,1)S(1)} custom-call(s32[1]{0:T(128)} %bitcast.rank_ref, f32[2]{0:T(128)S(1)} %copy-done.2, bf16[256,256]{1,0:T(8,128)(2,1)S(1)} %pad_maximum_fusion.queries_ref, bf16[2048,256]{1,0:T(8,128)(2,1)S(1)} %copy-done.1, f32[1,128]{1,0:T(1,128)S(1)} %bitcast.97), custom_call_target="tpu_custom_call" | custom-call | flops 1073741824 | bytes 1048576 | tf_op jit(solution)/shard_map/attention/pallas_call | solution.py:105
  93.8 2.6 %collective-permute-start.6 = (bf16[320,2048]{1,0:T(8,128)(2,1)}, bf16[320,2048]{1,0:T(8,128)(2,1)}, u32[]{:S(2)}, u32[]{:S(2)}) collective-permute-start(bf16[320,2048]{1,0:T(8,128)(2,1)} %collective-permute-done.5), channel_id=1, source_target_pairs={{0,1},{1,0},{2,3},{3,2},{4,5},{5,4},{6,7},{7,6},{8,9},{9,8},{10,11... | collective-permute-start | bytes 3932168 | tf_op jit(solution)/shard_map/ppermute | solution.py:124
  96.4 0.3 collective-permute-start.11
  96.7 0.7 collective-permute-start.9
  97.4 0.3 fusion.105
  97.7 1.6 collective-permute-done.6
  99.4 2.6 %fusion.22 = f32[320,256]{1,0:T(8,128)} fusion(bf16[320,2048]{1,0:T(8,128)(2,1)} %collective-permute-done.6, bf16[1,2048,256]{2,1,0:T(8,128)(2,1)S(1)} %copy-done.11), kind=kOutput, calls=%fused_computation.47 | convolution fusion | flops 335544320 | bytes 2686976 | tf_op jit(solution)/shard_map/dot_general | solution.py:258
  102.0 4.4 %convolution_convert_fusion.1 = bf16[320,2048]{1,0:T(8,128)(2,1)} fusion(bf16[1,256,2048]{2,1,0:T(8,128)(2,1)S(1)} %copy-done, f32[320,256]{1,0:T(8,128)} %fusion.22, bf16[320,2048]{1,0:T(8,128)(2,1)} %collective-permute-done.6, bf16[1,2048,256]{2,1,0:T(8,128)(2,1)} %param.34), kind=kOutput, calls=%fused_computation.1 | convolution fusion | flops 672235520 | bytes 5046272 | tf_op jit(solution)/shard_map/dot_general | solution.py:260
  106.4 0.4 collective-permute-start.7
  106.7 0.7 select_reduce_fusion
  107.4 1.5 fusion.5
  108.9 0.7 collective-permute-done.11
  109.6 1.3 collective-permute-start.12
  110.9 2.9 %fusion.26 = f32[320,256]{1,0:T(8,128)} fusion(bf16[320,2048]{1,0:T(8,128)(2,1)} %collective-permute-done.3, bf16[1,2048,256]{2,1,0:T(8,128)(2,1)} %param.35), kind=kOutput, calls=%fused_computation.51 | convolution fusion | flops 335544320 | bytes 2686976 | tf_op jit(solution)/shard_map/dot_general | solution.py:258
  113.7 4.4 %convolution_convert_fusion.3 = bf16[320,2048]{1,0:T(8,128)(2,1)} fusion(bf16[1,256,2048]{2,1,0:T(8,128)(2,1)S(1)} %copy-done, f32[320,256]{1,0:T(8,128)} %fusion.26, bf16[320,2048]{1,0:T(8,128)(2,1)} %collective-permute-done.3, bf16[1,2048,256]{2,1,0:T(8,128)(2,1)} %param.34), kind=kOutput, calls=%fused_computation.4 | convolution fusion | flops 672235520 | bytes 5046272 | tf_op jit(solution)/shard_map/dot_general | solution.py:260
  118.1 2.8 %fusion.24 = f32[320,256]{1,0:T(8,128)} fusion(bf16[320,2048]{1,0:T(8,128)(2,1)} %collective-permute-done.5, bf16[1,2048,256]{2,1,0:T(8,128)(2,1)} %param.35), kind=kOutput, calls=%fused_computation.49 | convolution fusion | flops 335544320 | bytes 2686976 | tf_op jit(solution)/shard_map/dot_general | solution.py:258
  120.9 4.8 %add_convert_fusion.1 = bf16[320,2048]{1,0:T(8,128)(2,1)} fusion(bf16[320,2048]{1,0:T(8,128)(2,1)} %collective-permute-done.7, bf16[1,256,2048]{2,1,0:T(8,128)(2,1)S(1)} %copy-done, f32[320,256]{1,0:T(8,128)} %fusion.24, bf16[320,2048]{1,0:T(8,128)(2,1)} %collective-permute-done.5, bf16[1,2048,256]{2,1,0:T(8,128)(2,1)} %param.34), kind=kOutput, calls=%fused_computation.10 | convolution fusion | flops 674856960 | bytes 6356992 | tf_op jit(solution)/shard_map/dot_general | solution.py:260
  125.7 0.3 collective-permute-start.8
  126.0 2.0 fusion.106
  127.9 1.3 fusion.108
  129.3 2.4 %convolution_convert_fusion.5 = bf16[128,2048]{1,0:T(8,128)(2,1)} fusion(bf16[128,2048]{1,0:T(8,128)(2,1)S(1)} %copy-done.6, f32[128,128]{1,0:T(8,128)S(1)} %fusion.108, bf16[128,2048]{1,0:T(8,128)(2,1)} %collective-permute-done.12, bf16[2048,128]{1,0:T(8,128)(2,1)S(1)} %copy-done.7), kind=kOutput, calls=%fused_computation.14 | convolution fusion | flops 134578176 | bytes 2162688 | tf_op jit(solution)/shard_map/dot_general | solution.py:251
  131.7 0.8 collective-permute-start.13
  132.5 2.1 %fusion.36 = f32[320,256]{1,0:T(8,128)S(1)} fusion(bf16[320,2048]{1,0:T(8,128)(2,1)} %bitcast.5, bf16[1,2048,256]{2,1,0:T(8,128)(2,1)} %param.34), kind=kOutput, calls=%fused_computation.60 | convolution fusion | flops 335544320 | bytes 2686976 | tf_op jit(solution)/shard_map/dot_general | solution.py:257
  134.6 4.4 %fusion.1 = f32[320,2048]{1,0:T(8,128)} fusion(bf16[320,2048]{1,0:T(8,128)(2,1)} %bitcast.5, bf16[1,256,2048]{2,1,0:T(8,128)(2,1)S(1)} %copy-done, bf16[1,2048,256]{2,1,0:T(8,128)(2,1)S(1)} %copy-done.12, f32[320,256]{1,0:T(8,128)S(1)} %fusion.36), kind=kOutput, calls=%fused_computation.6 | convolution fusion | flops 672890880 | bytes 6356992 | tf_op jit(solution)/shard_map/dot_general | solution.py:260
  139.0 16.9 %collective-permute-done.8 = bf16[320,2048]{1,0:T(8,128)(2,1)} collective-permute-done((bf16[320,2048]{1,0:T(8,128)(2,1)}, bf16[320,2048]{1,0:T(8,128)(2,1)}, u32[]{:S(2)}, u32[]{:S(2)}) %collective-permute-start.8) | collective-permute-done | bytes 1310752 | tf_op jit(solution)/shard_map/ppermute | solution.py:124
  155.8 4.2 %add_convert_fusion = bf16[320,2048]{1,0:T(8,128)(2,1)} fusion(bf16[320,2048]{1,0:T(8,128)(2,1)} %collective-permute-done.8, f32[320,2048]{1,0:T(8,128)} %fusion.1, bf16[320,2048]{1,0:T(8,128)(2,1)} %collective-permute-done.4), kind=kLoop, calls=%fused_computation.9 | loop fusion | flops 3276800 | bytes 6553600 | tf_op jit(solution)/shard_map/convert_element_type | solution.py:275
  160.0 5.4 %all-to-all-start.1 = ((bf16[8,40,2048]{2,1,0:T(8,128)(2,1)}), bf16[8,40,2048]{2,1,0:T(8,128)(2,1)S(1)}, u32[]{:S(2)}, u32[]{:S(2)}) async-start(bf16[8,40,2048]{2,1,0:T(8,128)(2,1)} %bitcast.101), calls=%async_computation.1 | async-start | bytes 2621440 | tf_op jit(solution)/shard_map/all_to_all | solution.py:276
  165.5 2.8 %convolution_convert_fusion.7 = bf16[128,2048]{1,0:T(8,128)(2,1)} fusion(bf16[128,2048]{1,0:T(8,128)(2,1)} %param.39, f32[128,128]{1,0:T(8,128)} %fusion.106, bf16[128,2048]{1,0:T(8,128)(2,1)} %collective-permute-done.9, bf16[2048,128]{1,0:T(8,128)(2,1)} %param.38), kind=kOutput, calls=%fused_computation.17 | convolution fusion | flops 134578176 | bytes 2162688 | tf_op jit(solution)/shard_map/dot_general | solution.py:251
  168.2 1.9 collective-permute-start.10
  170.2 2.1 %fusion.107 = f32[128,128]{1,0:T(8,128)} fusion(bf16[128,2048]{1,0:T(8,128)(2,1)} %collective-permute-done.11, bf16[2048,128]{1,0:T(8,128)(2,1)} %param.37), kind=kOutput, calls=%fused_computation.131 | convolution fusion | flops 67108864 | bytes 1114112 | tf_op jit(solution)/shard_map/dot_general | solution.py:248
  172.3 1.0 convolution_convert_fusion.9
  173.3 2.9 %add_convert_fusion.2 = bf16[128,2048]{1,0:T(8,128)(2,1)} fusion(bf16[128,2048]{1,0:T(8,128)(2,1)} %collective-permute-done.13, bf16[128,2048]{1,0:T(8,128)(2,1)} %param.39, f32[128,128]{1,0:T(8,128)} %fusion.107, bf16[128,2048]{1,0:T(8,128)(2,1)} %collective-permute-done.11, bf16[2048,128]{1,0:T(8,128)(2,1)} %param.38), kind=kOutput, calls=%fused_computation.62 | convolution fusion | flops 135626752 | bytes 2686976 | tf_op jit(solution)/shard_map/dot_general | solution.py:251
  176.1 0.3 collective-permute-start.14
  176.4 0.3 convolution_convert_fusion.11
  176.7 0.9 collective-permute-start
  177.6 1.2 add_convert_fusion.4
  178.8 1.3 collective-permute-start.2
  180.1 0.3 fusion.7
  180.4 14.5 %collective-permute-done.2 = bf16[64,2048]{1,0:T(8,128)(2,1)S(1)} collective-permute-done((bf16[64,2048]{1,0:T(8,128)(2,1)S(1)}, bf16[64,2048]{1,0:T(8,128)(2,1)S(1)}, u32[]{:S(2)}, u32[]{:S(2)}) %collective-permute-start.2) | collective-permute-done | bytes 262176 | tf_op jit(solution)/shard_map/ppermute | solution.py:124
  194.9 0.8 add_convert_fusion.3
  195.7 1.5 fusion.62
  197.3 2.5 %fusion.3 = bf16[128,2048]{1,0:T(8,128)(2,1)} fusion(f32[128,2048]{1,0:T(8,128)S(1)} %fusion.62, bf16[320,2048]{1,0:T(8,128)(2,1)S(1)} %bitcast.99, bf16[128,2048]{1,0:T(8,128)(2,1)} %collective-permute-done.14, f32[128,2048]{1,0:T(8,128)S(1)} %copy-done.8, bf16[128,2048]{1,0:T(8,128)(2,1)} %collective-permute-done.10, f32[128,320]{0,1:T(8,128)S(1)} %copy-done.10), kind=kOutput, calls=%fused_computation.13 | convolution fusion | flops 169689088 | bytes 5144576 | tf_op jit(solution)/shard_map/dot_general | solution.py:294
  (65 shorter events, 0.7 us)
Async XLA Ops:
  7.2 94.8 %copy-start = (bf16[1,256,2048]{2,1,0:T(8,128)(2,1)S(1)}, bf16[1,256,2048]{2,1,0:T(8,128)(2,1)}, u32[]{:S(2)}) copy-start(bf16[1,256,2048]{2,1,0:T(8,128)(2,1)} %param.36) | copy-start | bytes 3145732
  9.8 2.0 copy-start.13
  9.9 2.0 copy-start.17
  9.9 2.0 copy-start.18
  12.6 2.8 %copy-start.15 = (s32[128,2]{0,1:T(2,128)S(1)}, s32[128,2]{0,1:T(2,128)}, u32[]{:S(2)}) copy-start(s32[128,2]{0,1:T(2,128)} %param.32) | copy-start | bytes 3076
  12.6 2.9 %copy-start.9 = (bf16[128,2048]{1,0:T(8,128)(2,1)S(1)}, bf16[128,2048]{1,0:T(8,128)(2,1)}, u32[]{:S(2)}) copy-start(bf16[128,2048]{1,0:T(8,128)(2,1)} %param.30) | copy-start | bytes 1572868
  12.6 3.1 %copy-start.14 = (f32[2048]{0:T(1024)S(1)}, f32[2048]{0:T(1024)}, u32[]{:S(2)}) copy-start(f32[2048]{0:T(1024)} %param.31) | copy-start | bytes 24580
  18.2 39.5 %all-to-all-start = ((bf16[8,40,2048]{2,1,0:T(8,128)(2,1)}), bf16[8,40,2048]{2,1,0:T(8,128)(2,1)}, u32[]{:S(2)}, u32[]{:S(2)}) async-start(bf16[8,40,2048]{2,1,0:T(8,128)(2,1)} %bitcast.100), calls=%async_computation | async-start | bytes 2621440 | tf_op jit(solution)/shard_map/all_to_all | solution.py:242
  23.6 50.3 %all-gather.2.cloned.1.call-start = ((), (), s32[]{:S(2)}) async-start(), calls=%async_computation.2 | async-start | bytes 1179648 | tf_op jit(solution)/shard_map/all_gather | solution.py:204
  57.7 36.1 %collective-permute-start.5 = (bf16[320,2048]{1,0:T(8,128)(2,1)}, bf16[320,2048]{1,0:T(8,128)(2,1)}, u32[]{:S(2)}, u32[]{:S(2)}) collective-permute-start(bf16[320,2048]{1,0:T(8,128)(2,1)} %bitcast.5), channel_id=1, source_target_pairs={{0,2},{1,3},{2,0},{3,1},{4,6},{5,7},{6,4},{7,5},{8,10},{9,11},{10,... | collective-permute-start | bytes 3932168 | tf_op jit(solution)/shard_map/ppermute | solution.py:124
  59.5 14.4 %copy-start.2 = (f32[2]{0:T(128)S(1)}, f32[2]{0:T(128)}, u32[]{:S(2)}) copy-start(f32[2]{0:T(128)} %lambdas_ref.1) | copy-start | bytes 28
  59.5 14.4 %copy-start.3 = (f32[128]{0:T(128)S(1)}, f32[128]{0:T(128)}, u32[]{:S(2)}) copy-start(f32[128]{0:T(128)} %param.28) | copy-start | bytes 1540
  73.9 1.2 copy-start.1
  75.1 22.3 %copy-start.5 = (bf16[2048,128]{1,0:T(8,128)(2,1)S(1)}, bf16[2048,128]{1,0:T(8,128)(2,1)}, u32[]{:S(2)}) copy-start(bf16[2048,128]{1,0:T(8,128)(2,1)} %param.37) | copy-start | bytes 1572868
  75.1 24.2 %copy-start.11 = (bf16[1,2048,256]{2,1,0:T(8,128)(2,1)S(1)}, bf16[1,2048,256]{2,1,0:T(8,128)(2,1)}, u32[]{:S(2)}) copy-start(bf16[1,2048,256]{2,1,0:T(8,128)(2,1)} %param.35) | copy-start | bytes 3145732
  93.8 5.6 %collective-permute-start.6 = (bf16[320,2048]{1,0:T(8,128)(2,1)}, bf16[320,2048]{1,0:T(8,128)(2,1)}, u32[]{:S(2)}, u32[]{:S(2)}) collective-permute-start(bf16[320,2048]{1,0:T(8,128)(2,1)} %collective-permute-done.5), channel_id=1, source_target_pairs={{0,1},{1,0},{2,3},{3,2},{4,5},{5,4},{6,7},{7,6},{8,9},{9,8},{10,11... | collective-permute-start | bytes 3932168 | tf_op jit(solution)/shard_map/ppermute | solution.py:124
  96.4 14.5 %collective-permute-start.3 = (bf16[320,2048]{1,0:T(8,128)(2,1)}, bf16[320,2048]{1,0:T(8,128)(2,1)}, u32[]{:S(2)}, u32[]{:S(2)}) collective-permute-start(bf16[320,2048]{1,0:T(8,128)(2,1)} %bitcast.5), channel_id=1, source_target_pairs={{0,1},{1,0},{2,3},{3,2},{4,5},{5,4},{6,7},{7,6},{8,9},{9,8},{10,11... | collective-permute-start | bytes 3932168 | tf_op jit(solution)/shard_map/ppermute | solution.py:124
  96.4 13.2 %collective-permute-start.11 = (bf16[128,2048]{1,0:T(8,128)(2,1)S(1)}, bf16[128,2048]{1,0:T(8,128)(2,1)}, u32[]{:S(2)}, u32[]{:S(2)}) collective-permute-start(bf16[128,2048]{1,0:T(8,128)(2,1)S(1)} %fusion.15), channel_id=1, source_target_pairs={{0,2},{1,3},{2,0},{3,1},{4,6},{5,7},{6,4},{7,5},{8,10},{9,11},{10,... | collective-permute-start | bytes 1572872 | tf_op jit(solution)/shard_map/ppermute | solution.py:124
  96.7 29.3 %collective-permute-start.9 = (bf16[128,2048]{1,0:T(8,128)(2,1)S(1)}, bf16[128,2048]{1,0:T(8,128)(2,1)}, u32[]{:S(2)}, u32[]{:S(2)}) collective-permute-start(bf16[128,2048]{1,0:T(8,128)(2,1)S(1)} %fusion.15), channel_id=1, source_target_pairs={{0,1},{1,0},{2,3},{3,2},{4,5},{5,4},{6,7},{7,6},{8,9},{9,8},{10,11... | collective-permute-start | bytes 1572872 | tf_op jit(solution)/shard_map/ppermute | solution.py:124
  101.9 4.8 %copy-start.16 = (f32[128,2]{0,1:T(2,128)S(1)}, f32[128,2]{0,1:T(2,128)}, u32[]{:S(2)}) copy-start(f32[128,2]{0,1:T(2,128)} %param.33) | copy-start | bytes 3076
  101.9 5.5 %copy-start.6 = (bf16[128,2048]{1,0:T(8,128)(2,1)S(1)}, bf16[128,2048]{1,0:T(8,128)(2,1)}, u32[]{:S(2)}) copy-start(bf16[128,2048]{1,0:T(8,128)(2,1)} %param.39) | copy-start | bytes 1572868
  101.9 5.5 %copy-start.7 = (bf16[2048,128]{1,0:T(8,128)(2,1)S(1)}, bf16[2048,128]{1,0:T(8,128)(2,1)}, u32[]{:S(2)}) copy-start(bf16[2048,128]{1,0:T(8,128)(2,1)} %param.38) | copy-start | bytes 1572868
  106.4 14.6 %collective-permute-start.7 = (bf16[320,2048]{1,0:T(8,128)(2,1)}, bf16[320,2048]{1,0:T(8,128)(2,1)}, u32[]{:S(2)}, u32[]{:S(2)}) collective-permute-start(bf16[320,2048]{1,0:T(8,128)(2,1)} %convolution_convert_fusion.1), channel_id=1, source_target_pairs={{0,1},{1,0},{2,3},{3,2},{4,5},{5,4},{6,7},{7,6},{8,9},{9,8},{10,11... | collective-permute-start | bytes 3932168 | tf_op jit(solution)/shard_map/ppermute | solution.py:124
  109.6 18.4 %collective-permute-start.12 = (bf16[128,2048]{1,0:T(8,128)(2,1)}, bf16[128,2048]{1,0:T(8,128)(2,1)}, u32[]{:S(2)}, u32[]{:S(2)}) collective-permute-start(bf16[128,2048]{1,0:T(8,128)(2,1)} %collective-permute-done.11), channel_id=1, source_target_pairs={{0,1},{1,0},{2,3},{3,2},{4,5},{5,4},{6,7},{7,6},{8,9},{9,8},{10,11... | collective-permute-start | bytes 1572872 | tf_op jit(solution)/shard_map/ppermute | solution.py:124
  120.9 18.0 %collective-permute-start.4 = (bf16[320,2048]{1,0:T(8,128)(2,1)}, bf16[320,2048]{1,0:T(8,128)(2,1)}, u32[]{:S(2)}, u32[]{:S(2)}) collective-permute-start(bf16[320,2048]{1,0:T(8,128)(2,1)} %convolution_convert_fusion.3), channel_id=1, source_target_pairs={{0,1},{1,0},{2,3},{3,2},{4,5},{5,4},{6,7},{7,6},{8,9},{9,8},{10,11... | collective-permute-start | bytes 3932168 | tf_op jit(solution)/shard_map/ppermute | solution.py:124
  125.7 30.1 %collective-permute-start.8 = (bf16[320,2048]{1,0:T(8,128)(2,1)}, bf16[320,2048]{1,0:T(8,128)(2,1)}, u32[]{:S(2)}, u32[]{:S(2)}) collective-permute-start(bf16[320,2048]{1,0:T(8,128)(2,1)} %add_convert_fusion.1), channel_id=1, source_target_pairs={{0,2},{1,3},{2,0},{3,1},{4,6},{5,7},{6,4},{7,5},{8,10},{9,11},{10,... | collective-permute-start | bytes 3932168 | tf_op jit(solution)/shard_map/ppermute | solution.py:124
  131.7 2.9 %copy-start.12 = (bf16[1,2048,256]{2,1,0:T(8,128)(2,1)S(1)}, bf16[1,2048,256]{2,1,0:T(8,128)(2,1)}, u32[]{:S(2)}) copy-start(bf16[1,2048,256]{2,1,0:T(8,128)(2,1)} %param.35) | copy-start | bytes 3145732
  131.7 41.6 %collective-permute-start.13 = (bf16[128,2048]{1,0:T(8,128)(2,1)}, bf16[128,2048]{1,0:T(8,128)(2,1)}, u32[]{:S(2)}, u32[]{:S(2)}) collective-permute-start(bf16[128,2048]{1,0:T(8,128)(2,1)} %convolution_convert_fusion.5), channel_id=1, source_target_pairs={{0,1},{1,0},{2,3},{3,2},{4,5},{5,4},{6,7},{7,6},{8,9},{9,8},{10,11... | collective-permute-start | bytes 1572872 | tf_op jit(solution)/shard_map/ppermute | solution.py:124
  160.0 35.7 %all-to-all-start.1 = ((bf16[8,40,2048]{2,1,0:T(8,128)(2,1)}), bf16[8,40,2048]{2,1,0:T(8,128)(2,1)S(1)}, u32[]{:S(2)}, u32[]{:S(2)}) async-start(bf16[8,40,2048]{2,1,0:T(8,128)(2,1)} %bitcast.101), calls=%async_computation.1 | async-start | bytes 2621440 | tf_op jit(solution)/shard_map/all_to_all | solution.py:276
  165.5 6.8 %copy-start.4 = (bf16[256,2048]{1,0:T(8,128)(2,1)S(1)}, bf16[256,2048]{1,0:T(8,128)(2,1)}, u32[]{:S(2)}) copy-start(bf16[256,2048]{1,0:T(8,128)(2,1)} %param.29) | copy-start | bytes 3145732
  168.2 29.0 %collective-permute-start.10 = (bf16[128,2048]{1,0:T(8,128)(2,1)}, bf16[128,2048]{1,0:T(8,128)(2,1)}, u32[]{:S(2)}, u32[]{:S(2)}) collective-permute-start(bf16[128,2048]{1,0:T(8,128)(2,1)} %convolution_convert_fusion.7), channel_id=1, source_target_pairs={{0,1},{1,0},{2,3},{3,2},{4,5},{5,4},{6,7},{7,6},{8,9},{9,8},{10,11... | collective-permute-start | bytes 1572872 | tf_op jit(solution)/shard_map/ppermute | solution.py:124
  173.3 4.3 %collective-permute-start.1 = (bf16[64,2048]{1,0:T(8,128)(2,1)}, bf16[64,2048]{1,0:T(8,128)(2,1)}, u32[]{:S(2)}, u32[]{:S(2)}) collective-permute-start(bf16[64,2048]{1,0:T(8,128)(2,1)} %convolution_convert_fusion.9), channel_id=1, source_target_pairs={{0,1},{1,0},{2,3},{3,2},{4,5},{5,4},{6,7},{7,6},{8,9},{9,8},{10,11... | collective-permute-start | bytes 786440 | tf_op jit(solution)/shard_map/ppermute | solution.py:124
  176.1 21.1 %collective-permute-start.14 = (bf16[128,2048]{1,0:T(8,128)(2,1)}, bf16[128,2048]{1,0:T(8,128)(2,1)}, u32[]{:S(2)}, u32[]{:S(2)}) collective-permute-start(bf16[128,2048]{1,0:T(8,128)(2,1)} %add_convert_fusion.2), channel_id=1, source_target_pairs={{0,2},{1,3},{2,0},{3,1},{4,6},{5,7},{6,4},{7,5},{8,10},{9,11},{10,... | collective-permute-start | bytes 1572872 | tf_op jit(solution)/shard_map/ppermute | solution.py:124
  176.7 3.7 %collective-permute-start = (bf16[64,2048]{1,0:T(8,128)(2,1)S(1)}, bf16[64,2048]{1,0:T(8,128)(2,1)S(1)}, u32[]{:S(2)}, u32[]{:S(2)}) collective-permute-start(bf16[64,2048]{1,0:T(8,128)(2,1)S(1)} %convolution_convert_fusion.11), channel_id=1, source_target_pairs={{0,1},{1,0},{2,3},{3,2},{4,5},{5,4},{6,7},{7,6},{8,9},{9,8},{10,11... | collective-permute-start | bytes 786440 | tf_op jit(solution)/shard_map/ppermute | solution.py:124
  178.8 16.1 %collective-permute-start.2 = (bf16[64,2048]{1,0:T(8,128)(2,1)S(1)}, bf16[64,2048]{1,0:T(8,128)(2,1)S(1)}, u32[]{:S(2)}, u32[]{:S(2)}) collective-permute-start(bf16[64,2048]{1,0:T(8,128)(2,1)S(1)} %add_convert_fusion.4), channel_id=1, source_target_pairs={{0,2},{1,3},{2,0},{3,1},{4,6},{5,7},{6,4},{7,5},{8,10},{9,11},{10,... | collective-permute-start | bytes 786440 | tf_op jit(solution)/shard_map/ppermute | solution.py:124
  195.7 1.5 copy-start.8
  195.7 1.5 copy-start.10
Sparse Core Ops, SparseCore 0:
  27.1 46.7 all-gather.1
where the time goes:
time: 211 us; the launch traced here: 207 us
  waiting for transfers between devices  80.6 us (38%)
  matrix products  59 us (28%)
  starting transfers between devices  21.8 us (10%)
  Pallas kernels  18.6 us (9%)
  between operations  14.4 us (7%)
  other arithmetic  9.13 us (4%)
  local copies, waits for them, and re-layouts  3.11 us (1%)
    ppermute x15, waiting for transfers between devices, swap(): return lax.ppermute(rows, axis, [(i, i ^ distance) for i in range(size)])  33.8 us
    all_to_all x1, waiting for transfers between devices, body(): lax.all_to_all(outgoing, 'ep', split_axis=0, concat_axis=0, tiled=True)  33.4 us
    pallas_call x1, Pallas kernels, attention(): pl.pallas_call(functools.partial(attention_kernel, (rows, chunk, local_kv...  18.6 us
    dot_general x4, matrix products, routed_expert(): jnp.dot(hidden, expert_down[0], preferred_element_type=jnp.float32)  17.9 us
    all_gather x1, waiting for transfers between devices, body(): arrived = lax.all_gather(key_values, 'ep', axis=0, tiled=True)  12.8 us
    ppermute x15, starting transfers between devices, swap(): return lax.ppermute(rows, axis, [(i, i ^ distance) for i in range(size)])  10.9 us
    dot_general x4, matrix products, shared_expert(): jnp.dot(hidden, shared_down, preferred_element_type=jnp.float32)  9.5 us
    dot_general x3, matrix products, routed_expert(): lifted = jnp.dot(rows, expert_up[0], preferred_element_type=jnp.float32)  8.27 us
  transfers between devices with their start and end apart: 18, of which 6 were waited for; matrix products, arithmetic and copies ran while one was open for 27% of the time, Pallas kernels for 9%

commit v1 on v0

--- a/solution.py
+++ b/solution.py
@@ -155,7 +155,7 @@
     return sums[0]
 
 
-def body(
+def general_body(
     mixer_input,
     mixer_gain,
     query_one,
@@ -298,6 +298,801 @@
     return (mixer_sum, expert_output)
 
 
+def chunk_order(half):
+    order = [("n", 0)]
+    near = [("n", d) for d in range(1, half)]
+    far = [("f", d) for d in range(half)]
+    while near or far:
+        if far:
+            order.append(far.pop(0))
+        if near and (len(order) > 2 or not far):
+            order.append(near.pop(0))
+    return order
+
+
+def padded(rows):
+    return -(-rows // 16) * 16
+
+
+class Sizes:
+    def __init__(self, ep, tp, rows, width, tokens, hidden, shared, capacity, value_dim):
+        self.ep, self.tp, self.rows, self.width = ep, tp, rows, width
+        self.tokens, self.hidden, self.shared = tokens, hidden, shared
+        self.cap, self.stride = capacity, padded(capacity)
+        self.value_dim = value_dim
+        self.half = ep // 2
+        self.own = rows // tp
+        self.tile = min(512, width)
+
+    def names(self):
+        half, ep = self.half, self.ep
+        groups = (
+            [("XY", 0), ("INFO", 0), ("XC", 0), ("XC", 1)]
+            + [("FAR", d) for d in range(half)]
+            + [("NEAR", d, a) for d in range(1, half) for a in range(2)]
+            + [("FY", d) for d in range(half)]
+            + [("NRET", d) for d in range(1, half)]
+            + [("FRET", d) for d in range(half)]
+            + [("SC", 0), ("SC", 1), ("AY", 0), ("KVF", 0), ("OC", 0), ("OY", 0)]
+            + [("KVN", d) for d in range(1, half)]
+            + [("KVC", d) for d in range(1, half)]
+        )
+        table = {name: number for number, name in enumerate(groups)}
+        first = len(groups)
+        table["RC"], table["PC"], table["QY"] = first, first + ep, first + 2 * ep
+        return table, first + 3 * ep
+
+    def scratch(self):
+        bf, f32 = jnp.bfloat16, jnp.float32
+        ep, half, width, stride = self.ep, self.half, self.width, self.stride
+        tokens, rows, hidden, shared = self.tokens, self.rows, self.hidden, self.shared
+        vd = self.value_dim
+        return dict(
+            mx=((rows, width), bf),
+            wq=((width, 4 * HEAD), bf),
+            wk1=((width, HEAD), bf),
+            wk2=((width, HEAD), bf),
+            wv=((width, vd), bf),
+            wo=((2 * vd, width), bf),
+            wg=((width, hidden), bf),
+            wu=((width, hidden), bf),
+            wd=((hidden, width), bf),
+            sg=((width, shared), bf),
+            su=((width, shared), bf),
+            sd=((shared, width), bf),
+            xb=((2, 2, tokens, width), bf),
+            other=((8, tokens), f32),
+            outf=((half, stride, width), bf),
+            outn=((half, 2, stride, width), bf),
+            r=((ep, 2, 2, stride, width), bf),
+            p=((ep, 2, 2, stride, width), bf),
+            pr=((ep, 2, stride, width), bf),
+            q=((ep, 2, stride, width), bf),
+            qr=((ep, stride, width), bf),
+            fb=((ep, stride, width), bf),
+            tn=((2, half, stride, width), bf),
+            tf=((half, stride, width), bf),
+            s=((2, 2, tokens, width), bf),
+            sr=((2, tokens, width), bf),
+            ao=((tokens, width), bf),
+            ar=((tokens, width), bf),
+            acc=((tokens, width), f32),
+            wown=((2, 2, tokens, half * stride), bf),
+            woth=((2, tokens, half * stride), bf),
+            nm=((rows, width), bf),
+            qs=((2, 2, rows, 2 * HEAD), bf),
+            kv=((ep, rows, 2 * HEAD + vd), bf),
+            sc=((2, ep, rows, rows), f32),
+            stat=((2, rows, 128), f32),
+            tot=((2, rows, 128), f32),
+            pv=((2, rows, vd), f32),
+            hr=((rows, 2 * vd), bf),
+            o=((2, 2, self.own, width), bf),
+            orx=((2, self.own, width), bf),
+            oq=((2, self.own, width), bf),
+            oy=((self.own, width), bf),
+        )
+
+    def vmem_bytes(self):
+        total = 0
+        for shape, dtype in self.scratch().values():
+            size = jnp.dtype(dtype).itemsize
+            for extent in shape[:-1]:
+                size *= extent
+            total += size * (-(-shape[-1] // 128) * 128)
+        return total
+
+
+class Later:
+    def __init__(self, start):
+        self.start = start
+
+
+def fused_kernel(sizes, keys, *refs):
+    (lam, info, x, xgain, mgain, hgain) = refs[:6]
+    (h_mx, h_q1, h_q2, h_k1, h_k2, h_v, h_wo, h_g, h_u, h_d, h_sg, h_su, h_sd) = refs[6:19]
+    mix_out, exp_out = refs[19:21]
+    b = dict(zip(keys, refs[21 : 21 + len(keys)]))
+    send_sem, recv_sem, load_sem = refs[21 + len(keys) :]
+    half, ep, width, stride, cap = sizes.half, sizes.ep, sizes.width, sizes.stride, sizes.cap
+    tokens, rows, tile, vd = sizes.tokens, sizes.rows, sizes.tile, sizes.value_dim
+    f32, bf = jnp.float32, jnp.bfloat16
+    table, _ = sizes.names()
+    order = chunk_order(half)
+    place = {name: number for number, name in enumerate(order)}
+
+    me = lax.axis_index("ep")
+    tp = lax.axis_index("tp")
+    side = me // half
+    spot = me % half
+    row_of = tp // 2
+    core = tp % 2
+    tiles = width // tile
+
+    near_to = [side * half + (spot + d) % half for d in range(half)]
+    near_by = [side * half + (spot + half - d) % half for d in range(half)]
+    far_to = [(1 - side) * half + (spot + d) % half for d in range(half)]
+    far_by = [(1 - side) * half + (spot + half - d) % half for d in range(half)]
+
+    def near(d):
+        return (near_to[d], tp)
+
+    def near_from(d):
+        return (near_by[d], tp)
+
+    def far(d):
+        return (far_to[d], tp)
+
+    def far_from(d):
+        return (far_by[d], tp)
+
+    partner_y = (me, (1 - row_of) * 2 + core)
+    partner_c = (me, row_of * 2 + 1 - core)
+
+    def remote(number, source, target, device):
+        return pltpu.make_async_remote_copy(
+            src_ref=source,
+            dst_ref=target,
+            send_sem=send_sem.at[number],
+            recv_sem=recv_sem.at[number],
+            device_id=device,
+            device_id_type=pl.DeviceIdType.MESH,
+        )
+
+    copies = {}
+
+    def made(name):
+        source, target, device = copies[name]
+        return remote(table[name], source(), target(), device)
+
+    def copy(name, source, target, device):
+        copies[name] = (source, target, device)
+        return Later(lambda: made(name).start())
+
+    def dot(left, right):
+        return jnp.dot(left, right, preferred_element_type=f32)
+
+    loads = {}
+    pairs = dict(
+        mx=(h_mx, b["mx"]),
+        q1=(h_q1, b["wq"].at[:, : 2 * HEAD]),
+        q2=(h_q2, b["wq"].at[:, 2 * HEAD :]),
+        k1=(h_k1, b["wk1"]),
+        k2=(h_k2, b["wk2"]),
+        v=(h_v, b["wv"]),
+        sg=(h_sg, b["sg"]),
+        su=(h_su, b["su"]),
+        sd=(h_sd, b["sd"]),
+        wg=(h_g.at[0], b["wg"]),
+        wu=(h_u.at[0], b["wu"]),
+        wd=(h_d.at[0], b["wd"]),
+        wo=(h_wo, b["wo"]),
+    )
+    for number, (name, (source, target)) in enumerate(pairs.items()):
+        loads[name] = pltpu.make_async_copy(source, target, load_sem.at[number])
+        loads[name].start()
+
+    barrier = pltpu.get_barrier_semaphore()
+    peers = [near(d) for d in range(1, half)] + [far(d) for d in range(half)]
+    peers += [partner_y, partner_c]
+    for device in peers:
+        pl.semaphore_signal(
+            barrier, inc=1, device_id=device, device_id_type=pl.DeviceIdType.MESH
+        )
+
+    def norm_rows(source, target, count, gain):
+        step = min(32, count)
+
+        @pl.loop(0, count // step)
+        def _(index):
+            at = pl.ds(pl.multiple_of(index * step, step), step)
+            values = source[at, :].astype(f32)
+            factor = lax.rsqrt(jnp.mean(values * values, axis=-1, keepdims=True) + EPS)
+            target[at, :] = (values * factor * gain[...]).astype(bf)
+
+    norm_rows(x, b["xb"].at[0, 0], tokens, xgain)
+
+    earlier = (
+        lax.broadcasted_iota(jnp.int32, (tokens, tokens), 0)
+        < lax.broadcasted_iota(jnp.int32, (tokens, tokens), 1)
+    ).astype(bf)
+    padded_ep = -(-ep // 8) * 8
+    relative = lax.broadcasted_iota(jnp.int32, (padded_ep, tokens), 0)
+    in_far = relative >= half
+    turn = jnp.where(in_far, relative - half, relative) + spot
+    turn = jnp.where(turn >= half, turn - half, turn)
+    names_half = jnp.where(in_far, 1 - side, side)
+    expert = (names_half * half + turn).astype(f32)
+
+    def routing(info_ref):
+        first = info_ref[0:1, :] == expert
+        second = info_ref[1:2, :] == expert
+        named = jnp.where(first | second, 1.0, 0.0)
+        position = dot(named.astype(bf), earlier)
+        position = jnp.where(named > 0.0, position, -1.0)
+        weight = jnp.where(first, info_ref[2:3, :], 0.0) + jnp.where(second, info_ref[3:4, :], 0.0)
+        return position, weight
+
+    slot = lax.broadcasted_iota(jnp.int32, (stride, tokens), 0).astype(f32)
+
+    def chosen(position, which):
+        return slot == position[which : which + 1, :]
+
+    def select(position, which):
+        return jnp.concatenate(
+            [jnp.where(chosen(position, k), 1.0, 0.0) for k in which], axis=0
+        ).astype(bf)
+
+    def spread(position, weight, which):
+        stacked = jnp.concatenate(
+            [jnp.where(chosen(position, k), weight[k : k + 1, :], 0.0) for k in which], axis=0
+        )
+        turned = stacked.T
+        upper = turned.astype(bf)
+        return upper, (turned - upper.astype(f32)).astype(bf)
+
+    own_place, own_weight = routing(info)
+    near_set = list(range(half))
+    far_set = list(range(half, 2 * half))
+    select_near = select(own_place, near_set)
+    select_far = select(own_place, far_set)
+
+    pl.semaphore_wait(barrier, len(peers))
+    copy(("XY", 0), lambda: b["xb"].at[0, 0], lambda: b["xb"].at[1, 0], partner_y).start()
+    copy(("INFO", 0), lambda: info, lambda: b["other"], partner_y).start()
+    copy(("XC", 0), lambda: b["xb"].at[0, 0], lambda: b["xb"].at[0, 1], partner_c).start()
+
+    def pick(select_rows, source, store):
+        for n in range(tiles):
+            cols = slice(n * tile, (n + 1) * tile)
+            picked = dot(select_rows, source[:, cols]).astype(bf)
+            for d in range(half):
+                store(d, cols, picked[d * stride : (d + 1) * stride, :])
+
+    def store_near(a):
+        def store(d, cols, value):
+            b["outn"][d, a, :, cols] = value
+
+        return store
+
+    def store_far(d, cols, value):
+        b["outf"][d, :, cols] = value
+
+    pick(select_near, b["xb"].at[0, 0], store_near(0))
+
+    def start_near(a):
+        for d in range(1, half):
+            copy(
+                ("NEAR", d, a),
+                lambda d=d: b["outn"].at[d, a, pl.ds(0, cap)],
+                lambda d=d: b["r"].at[place[("n", d)], 0, a, pl.ds(0, cap)],
+                near(d),
+            ).start()
+
+    start_near(0)
+    pick(select_far, b["xb"].at[0, 0], store_far)
+
+    def start_far(d):
+        copy(
+            ("FAR", d),
+            lambda: b["outf"].at[d, pl.ds(0, cap)],
+            lambda: b["r"].at[place[("f", d)], 0, 0, pl.ds(0, cap)],
+            far(d),
+        ).start()
+
+    for d in range(half // 2):
+        start_far(d)
+
+    loads["mx"].wait()
+    norm_rows(b["mx"], b["nm"], rows, mgain)
+    for name in ("q1", "q2", "k1", "k2", "v"):
+        loads[name].wait()
+    lane = lax.broadcasted_iota(jnp.int32, (rows, 2 * HEAD), 1)
+    b["kv"][me, :, 0:HEAD] = dot(b["nm"][...], b["wk1"][...]).astype(bf)
+    b["kv"][me, :, HEAD : 2 * HEAD] = dot(b["nm"][...], b["wk2"][...]).astype(bf)
+    b["kv"][me, :, 2 * HEAD :] = dot(b["nm"][...], b["wv"][...]).astype(bf)
+
+    copy(("KVF", 0), lambda: b["kv"].at[me], lambda: b["kv"].at[me], far(0))
+
+    @pl.when(side == 0)
+    def _():
+        made(("KVF", 0)).start()
+
+    for d in range(1, half):
+        copy(("KVN", d), lambda: b["kv"].at[me], lambda: b["kv"].at[me], near(d))
+
+        @pl.when(near_to[d] > me)
+        def _(d=d):
+            made(("KVN", d)).start()
+
+    for d in range(half // 2, half):
+        start_far(d)
+
+    for m in range(2):
+        queries = dot(b["nm"][...], b["wq"][:, m * 2 * HEAD : (m + 1) * 2 * HEAD])
+        turned = pltpu.roll(queries, HEAD, 1)
+        keep = (lane < HEAD) if m == 0 else (lane >= HEAD)
+        for g in range(2):
+            source = queries if g == m else turned
+            b["qs"][m, g] = jnp.where(keep, source, 0.0).astype(bf)
+
+    def shared_expert(a):
+        both = b["xb"][a].reshape(2 * tokens, width)
+        gated = dot(both, b["sg"][...])
+        lifted = dot(both, b["su"][...])
+        hidden = (jax.nn.silu(gated) * lifted).astype(bf)
+        for n in range(tiles):
+            cols = slice(n * tile, (n + 1) * tile)
+            part = dot(hidden, b["sd"][:, cols]).astype(bf)
+            b["s"][a, 0, :, cols] = part[:tokens]
+            b["s"][a, 1, :, cols] = part[tokens:]
+
+    for name in ("sg", "su", "sd"):
+        loads[name].wait()
+    made(("XC", 0)).wait_recv()
+    shared_expert(0)
+    copy(("SC", 0), lambda: b["s"].at[0, 1], lambda: b["sr"].at[0], partner_c).start()
+
+    made(("XY", 0)).wait_recv()
+    made(("INFO", 0)).wait_recv()
+    copy(("XC", 1), lambda: b["xb"].at[1, 0], lambda: b["xb"].at[1, 1], partner_c).start()
+    other_place, other_weight = routing(b["other"])
+    pick(select(other_place, near_set), b["xb"].at[1, 0], store_near(1))
+    start_near(1)
+    b["r"][0, 0] = b["outn"][0]
+
+    def core_forward(position):
+        return remote(
+            table["RC"] + position, b["r"].at[position, 0], b["r"].at[position, 1], partner_c
+        )
+
+    core_forward(0).start()
+    for which, (at, wt, group) in enumerate(
+        ((own_place, own_weight, near_set), (own_place, own_weight, far_set))
+    ):
+        upper, lower = spread(at, wt, group)
+        b["wown"][which, 0] = upper
+        b["wown"][which, 1] = lower
+    upper, lower = spread(other_place, other_weight, near_set)
+    b["woth"][0] = upper
+    b["woth"][1] = lower
+    for d in range(half):
+        b["tf"][d, cap:, :] = jnp.zeros((stride - cap, width), bf)
+        for a in range(2):
+            b["tn"][a, d, cap:, :] = jnp.zeros((stride - cap, width), bf)
+    made(("XC", 1)).wait_recv()
+    shared_expert(1)
+    copy(("SC", 1), lambda: b["s"].at[1, 1], lambda: b["sr"].at[1], partner_c).start()
+
+    for name in ("wg", "wu", "wd"):
+        loads[name].wait()
+
+    def arrive_far(d):
+        made(("FAR", d)).wait_recv()
+        made(("FY", d)).start()
+
+    def crossed(d):
+        made(("FY", d)).wait_recv()
+        core_forward(place[("f", d)]).start()
+
+    def arrive_near(d):
+        for a in range(2):
+            made(("NEAR", d, a)).wait_recv()
+        core_forward(place[("n", d)]).start()
+
+    def relay_kv():
+        @pl.when(side == 1)
+        def _():
+            slot_of = b["kv"].at[far_by[0]]
+            remote(table[("KVF", 0)], slot_of, slot_of, far(0)).wait_recv()
+
+        for d in range(1, half):
+            copy(("KVC", d), lambda: b["kv"].at[far_by[0]], lambda: b["kv"].at[far_by[0]], near(d))
+
+            @pl.when(side == 1)
+            def _(d=d):
+                made(("KVC", d)).start()
+
+    events = {}
+
+    def at_step(step, action):
+        events.setdefault(max(step, 0), []).append(action)
+
+    for position, (kind, d) in enumerate(order):
+        if kind == "f":
+            copies[("FY", d)] = (
+                lambda position=position: b["r"].at[position, 0, 0, pl.ds(0, cap)],
+                lambda position=position: b["r"].at[position, 0, 1, pl.ds(0, cap)],
+                partner_y,
+            )
+            at_step(position - 2, functools.partial(arrive_far, d))
+            at_step(position - 1, functools.partial(crossed, d))
+        elif d > 0:
+            at_step(position - 1, functools.partial(arrive_near, d))
+    at_step(3, relay_kv)
+
+    def is_one(value, choices):
+        found = value == choices[0]
+        for choice in choices[1:]:
+            found = jnp.logical_or(found, value == choice)
+        return found
+
+    far_places = [place[("f", d)] for d in range(half)]
+    row_count = 4 * stride
+
+    def back_copy(number):
+        return remote(
+            table["PC"] + number, b["p"].at[number, 1], b["pr"].at[number], partner_c
+        )
+
+    def cross_copy(number):
+        return remote(
+            table["QY"] + number,
+            b["q"].at[number, 1, pl.ds(0, cap)],
+            b["qr"].at[number, pl.ds(0, cap)],
+            partner_y,
+        )
+
+    def step_body(step, carry):
+        for when, actions in sorted(events.items()):
+
+            @pl.when(step == when)
+            def _(actions=actions):
+                for action in actions:
+                    action()
+
+        @pl.when(step < ep)
+        def _():
+            core_forward(step).wait_recv()
+            arrived = b["r"][step].reshape(row_count, width)
+            gated = dot(arrived, b["wg"][...])
+            lifted = dot(arrived, b["wu"][...])
+            hidden = (jax.nn.silu(gated) * lifted).astype(bf)
+
+            for n in range(tiles):
+                cols = slice(n * tile, (n + 1) * tile)
+                part = dot(hidden, b["wd"][:, cols]).astype(bf)
+                b["p"][step, :, :, :, cols] = part.reshape(2, 2, stride, tile)
+            back_copy(step).start()
+
+        last = step - 1
+
+        @pl.when(jnp.logical_and(last >= 0, last < ep))
+        def _():
+            back_copy(last).wait_recv()
+            for a in range(2):
+                b["q"][last, a] = (
+                    b["p"][last, 0, a].astype(f32) + b["pr"][last, a].astype(f32)
+                ).astype(bf)
+
+            @pl.when(last == 0)
+            def _():
+                for a in range(2):
+                    b["tn"][a, 0, 0:cap, :] = b["q"][0, a, 0:cap, :]
+
+            for d in range(1, half):
+                at = place[("n", d)]
+                copy(
+                    ("NRET", d),
+                    lambda at=at: b["q"].at[at, :, pl.ds(0, cap)],
+                    lambda d=d: b["tn"].at[:, d, pl.ds(0, cap)],
+                    near_from(d),
+                )
+
+                @pl.when(last == at)
+                def _(d=d):
+                    made(("NRET", d)).start()
+
+            @pl.when(is_one(last, far_places))
+            def _():
+                cross_copy(last).start()
+
+        older = step - 2
+
+        @pl.when(jnp.logical_and(older >= 0, is_one(older, far_places)))
+        def _():
+            cross_copy(older).wait_recv()
+            b["fb"][older] = (
+                b["q"][older, 0].astype(f32) + b["qr"][older].astype(f32)
+            ).astype(bf)
+            for d in range(half):
+                at = place[("f", d)]
+                copy(
+                    ("FRET", d),
+                    lambda at=at: b["fb"].at[at, pl.ds(0, cap)],
+                    lambda d=d: b["tf"].at[d, pl.ds(0, cap)],
+                    far_from(d),
+                )
+
+                @pl.when(older == at)
+                def _(d=d):
+                    made(("FRET", d)).start()
+
+        return carry
+
+    lax.fori_loop(0, ep + 2, step_body, 0)
+
+    def kv_arrival(name, source, d):
+        block = b["kv"].at[source]
+        remote(table[(name, d)], block, block, near(d)).wait_recv()
+
+    for d in range(1, half):
+
+        @pl.when(near_by[d] < me)
+        def _(d=d):
+            kv_arrival("KVN", near_by[d], d)
+
+        @pl.when(side == 1)
+        def _(d=d):
+            kv_arrival("KVC", (1 - side) * half + (spot + half - d) % half, d)
+
+    scale = HEAD**-0.5 * math.log2(math.e)
+    row_place = me * rows + lax.broadcasted_iota(jnp.int32, (rows, rows), 0)
+    col_place = lax.broadcasted_iota(jnp.int32, (rows, rows), 1)
+    halves = [slice(c * 128, (c + 1) * 128) for c in range(rows // 128)]
+
+    def head(g):
+        b["stat"][...] = jnp.full((2, rows, 128), NEG, f32)
+        b["tot"][...] = jnp.zeros((2, rows, 128), f32)
+        b["pv"][...] = jnp.zeros((2, rows, vd), f32)
+
+        def score(j, carry):
+            keys_j = b["kv"][j, :, 0 : 2 * HEAD]
+            for m in range(2):
+                scores = lax.dot_general(
+                    b["qs"][m, g], keys_j, (((1,), (1,)), ((), ())), preferred_element_type=f32
+                )
+                scores = jnp.where(j * rows + col_place <= row_place, scores, NEG)
+                b["sc"][m, j] = scores
+                most = b["stat"][m]
+                for cols in halves:
+                    most = jnp.maximum(most, scores[:, cols])
+                b["stat"][m] = most
+            return carry
+
+        lax.fori_loop(0, me + 1, score, 0)
+        for m in range(2):
+            most = jnp.max(b["stat"][m], axis=1, keepdims=True)
+            b["stat"][m] = jnp.broadcast_to(most, (rows, 128))
+
+        def weigh(j, carry):
+            values = b["kv"][j, :, 2 * HEAD :]
+            for m in range(2):
+                most = b["stat"][m]
+                total = b["tot"][m]
+                parts = []
+                for cols in halves:
+                    weights = jnp.exp2((b["sc"][m, j, :, cols] - most) * scale)
+                    total = total + weights
+                    parts.append(weights.astype(bf))
+                b["tot"][m] = total
+                b["pv"][m] += dot(jnp.concatenate(parts, axis=1), values)
+            return carry
+
+        lax.fori_loop(0, me + 1, weigh, 0)
+        sums = [jnp.sum(b["tot"][m], axis=1, keepdims=True) for m in range(2)]
+        combined = b["pv"][0] / sums[0] - lam[g] * (b["pv"][1] / sums[1])
+        factor = lax.rsqrt(jnp.mean(combined * combined, axis=1, keepdims=True) + EPS)
+        b["hr"][:, g * vd : (g + 1) * vd] = (combined * factor * hgain[...]).astype(bf)
+
+    for g in range(2):
+        head(g)
+
+    loads["wo"].wait()
+    own = sizes.own
+    for n in range(tiles):
+        cols = slice(n * tile, (n + 1) * tile)
+        part = dot(b["hr"][...], b["wo"][:, cols]).astype(bf)
+        b["o"][:, :, :, cols] = part.reshape(2, 2, own, tile)
+    copy(("OC", 0), lambda: b["o"].at[:, 1 - core], lambda: b["orx"], partner_c).start()
+
+    for d in range(1, half):
+        made(("NRET", d)).wait_recv()
+    for a in range(2):
+        made(("SC", a)).wait_recv()
+    for n in range(tiles):
+        cols = slice(n * tile, (n + 1) * tile)
+        back = b["tn"][1, :, :, cols].reshape(half * stride, tile)
+        total = dot(b["woth"][0], back) + dot(b["woth"][1], back)
+        total = total + b["s"][1, 0, :, cols].astype(f32) + b["sr"][1, :, cols].astype(f32)
+        b["ao"][:, cols] = total.astype(bf)
+    copy(("AY", 0), lambda: b["ao"], lambda: b["ar"], partner_y).start()
+
+    made(("OC", 0)).wait_recv()
+    for a in range(2):
+        b["oq"][a] = (b["o"][a, core].astype(f32) + b["orx"][a].astype(f32)).astype(bf)
+    copy(("OY", 0), lambda: b["oq"].at[1 - row_of], lambda: b["oy"], partner_y).start()
+
+    for n in range(tiles):
+        cols = slice(n * tile, (n + 1) * tile)
+        back = b["tn"][0, :, :, cols].reshape(half * stride, tile)
+        total = dot(b["wown"][0, 0], back) + dot(b["wown"][0, 1], back)
+        b["acc"][:, cols] = (
+            total + b["s"][0, 0, :, cols].astype(f32) + b["sr"][0, :, cols].astype(f32)
+        )
+    made(("OY", 0)).wait_recv()
+    mix_out[...] = (b["oq"][row_of].astype(f32) + b["oy"][...].astype(f32)).astype(bf)
+
+    for d in range(half):
+        made(("FRET", d)).wait_recv()
+    made(("AY", 0)).wait_recv()
+    for n in range(tiles):
+        cols = slice(n * tile, (n + 1) * tile)
+        back = b["tf"][:, :, cols].reshape(half * stride, tile)
+        total = dot(b["wown"][1, 0], back) + dot(b["wown"][1, 1], back)
+        total = total + b["acc"][:, cols] + b["ar"][:, cols].astype(f32)
+        exp_out[:, cols] = total.astype(bf)
+
+    conditional = {("KVF", 0): side == 0}
+    for d in range(1, half):
+        conditional[("KVN", d)] = near_to[d] > me
+        conditional[("KVC", d)] = side == 1
+    for name in copies:
+        if name in conditional:
+
+            @pl.when(conditional[name])
+            def _(name=name):
+                made(name).wait_send()
+
+        else:
+            made(name).wait_send()
+    for position in range(ep):
+        core_forward(position).wait_send()
+        back_copy(position).wait_send()
+        if position in far_places:
+            cross_copy(position).wait_send()
+
+
+def fused(sizes, args):
+    scratch = sizes.scratch()
+    keys = list(scratch)
+    _, count = sizes.names()
+    vmem = pl.BlockSpec(memory_space=pltpu.VMEM)
+    smem = pl.BlockSpec(memory_space=pltpu.SMEM)
+    hbm = pl.BlockSpec(memory_space=pltpu.HBM)
+    return pl.pallas_call(
+        functools.partial(fused_kernel, sizes, keys),
+        out_shape=(
+            jax.ShapeDtypeStruct((sizes.own, sizes.width), jnp.bfloat16),
+            jax.ShapeDtypeStruct((sizes.tokens, sizes.width), jnp.bfloat16),
+        ),
+        in_specs=[smem] + [vmem] * 5 + [hbm] * 13,
+        out_specs=(vmem, vmem),
+        scratch_shapes=[pltpu.VMEM(shape, dtype) for shape, dtype in scratch.values()]
+        + [
+            pltpu.SemaphoreType.DMA((count,)),
+            pltpu.SemaphoreType.DMA((count,)),
+            pltpu.SemaphoreType.DMA((13,)),
+        ],
+        compiler_params=pltpu.CompilerParams(
+            collective_id=0, has_side_effects=True, vmem_limit_bytes=VMEM_LIMIT
+        ),
+        name="layer",
+    )(*args)
+
+
+VMEM_LIMIT = 67043328
+
+
+def fused_body(sizes, *arrays):
+    (
+        mixer_input,
+        mixer_gain,
+        query_one,
+        query_two,
+        key_one,
+        key_two,
+        value_weight,
+        lambdas,
+        head_gain,
+        output_weight,
+        expert_input,
+        expert_gain,
+        routes,
+        route_weight,
+        expert_gate,
+        expert_up,
+        expert_down,
+        shared_gate,
+        shared_up,
+        shared_down,
+    ) = arrays
+    info = jnp.concatenate(
+        [
+            routes.T.astype(jnp.float32),
+            route_weight.T,
+            jnp.zeros((4, sizes.tokens), jnp.float32),
+        ],
+        axis=0,
+    )
+    return fused(
+        sizes,
+        (
+            lambdas,
+            info,
+            expert_input,
+            expert_gain.reshape(1, -1),
+            mixer_gain.reshape(1, -1),
+            head_gain.reshape(1, -1),
+            mixer_input,
+            query_one,
+            query_two,
+            key_one,
+            key_two,
+            value_weight,
+            output_weight,
+            expert_gate,
+            expert_up,
+            expert_down,
+            shared_gate,
+            shared_up,
+            shared_down,
+        ),
+    )
+
+
+def body(*arrays):
+    ep_size, tp_size = lax.axis_size("ep"), lax.axis_size("tp")
+    mixer_input, query_one, key_one = arrays[0], arrays[2], arrays[4]
+    head_gain, expert_input, routes = arrays[8], arrays[10], arrays[12]
+    expert_gate, shared_gate = arrays[14], arrays[17]
+    rows, width = mixer_input.shape
+    tokens, top_count = routes.shape
+    local_experts = expert_gate.shape[0]
+    capacity = max(2, 5 * tokens * top_count // (4 * local_experts * ep_size))
+    fits = (
+        tp_size == 4
+        and ep_size % 2 == 0
+        and ep_size >= 4
+        and local_experts == 1
+        and top_count == 2
+        and key_one.shape[1] == HEAD
+        and query_one.shape[1] == 2 * HEAD
+        and head_gain.shape[0] == 128
+        and tokens == 128
+        and rows % (16 * tp_size) == 0
+        and rows % 128 == 0
+        and width % 512 == 0
+        and expert_input.shape[1] == width
+        and capacity % 8 == 0
+    )
+    if fits:
+        sizes = Sizes(
+            ep_size,
+            tp_size,
+            rows,
+            width,
+            tokens,
+            expert_gate.shape[2],
+            shared_gate.shape[1],
+            capacity,
+            head_gain.shape[0],
+        )
+        if sizes.vmem_bytes() + 8 * 2**20 <= VMEM_LIMIT:
+            return fused_body(sizes, *arrays)
+    return general_body(*arrays)
+
+
 def solution(mesh):
     in_specs = (
         P("ep", None),

time: 211 us -> 111 us (0.53)
  the two profiles are of different devices: /device:TPU:31 before, /device:TPU:0 now
where the time goes in v1:
time: 111 us
  Pallas kernels  103 us (93%)
  local copies, waits for them, and re-layouts  6.88 us (6%)
    pallas_call x1, Pallas kernels, fused(): pl.pallas_call(functools.partial(fused_kernel, sizes, keys), out_shape=(j...  103 us
    unnamed x12, local copies, waits for them, and re-layouts  6.81 us

profile of v1, /device:TPU:0, one launch (start us, length us, event | category | flops | bytes accessed | tf_op | source)
XLA Modules:
  0.0 110.9 jit_solution(677665005869992161)
XLA Ops:
  0.6 0.0 copy-start.2
  0.7 0.1 pad.2.clone
  0.7 0.6 copy-done.2
  1.3 0.0 copy-start.3
  1.3 0.7 copy-done.3
  2.0 0.7 maximum_maximum_fusion.refs_1_
  2.7 0.0 copy-start.1
  2.7 2.0 %copy.22.refs_9_ = bf16[2048,64]{1,0:T(8,128)(2,1)} copy(bf16[2048,64]{0,1:T(8,128)(2,1)} %param.24) | data formatting | bytes 524288 | tf_op args[4]
  4.7 0.0 copy-done.1
  4.7 1.0 copy.23.refs_10_
  5.7 102.7 %layer.1 = (bf16[64,2048]{1,0:T(8,128)(2,1)}, bf16[128,2048]{1,0:T(8,128)(2,1)}) custom-call(f32[2]{0:T(128)} %refs_0_.1, f32[8,128]{1,0:T(8,128)} %maximum_maximum_fusion.refs_1_, bf16[128,2048]{1,0:T(8,128)(2,1)} %refs_2_.1, f32[1,2048]{1,0:T(1,128)} %bitcast.6, f32[1,2048]{1,0:T(1,128)} %bitcast.7, f32[1,128]{1,0:T(1,128)} %bitcast.9, ...), custom_call_target="tpu_custom_call" | custom-call | tf_op jit(solution)/shard_map/layer/pallas_call | solution.py:973
  108.4 0.0 copy-start
  108.4 1.7 %copy.26 = bf16[64,2048]{1,0:T(8,128)(2,1)} copy(bf16[64,2048]{1,0:T(8,128)(2,1)} %get-tuple-element.4) | data formatting | bytes 524288
  110.1 0.0 copy-done
  110.1 0.8 copy.27
  (2 shorter events, 0.0 us)
Async XLA Ops:
  0.6 0.7 copy-start.2
  1.3 0.7 copy-start.3
  2.7 2.0 %copy-start.1 = (bf16[2048,64]{0,1:T(8,128)(2,1)S(1)}, bf16[2048,64]{0,1:T(8,128)(2,1)}, u32[]{:S(2)}) copy-start(bf16[2048,64]{0,1:T(8,128)(2,1)} %param.25) | copy-start | bytes 786436
  108.4 1.7 %copy-start = (bf16[128,2048]{1,0:T(8,128)(2,1)S(1)}, bf16[128,2048]{1,0:T(8,128)(2,1)}, u32[]{:S(2)}) copy-start(bf16[128,2048]{1,0:T(8,128)(2,1)} %get-tuple-element.5) | copy-start | bytes 1572868

commit v2 on v1

--- a/solution.py
+++ b/solution.py
@@ -299,15 +299,10 @@
 
 
 def chunk_order(half):
-    order = [("n", 0)]
-    near = [("n", d) for d in range(1, half)]
+    near = [("n", d) for d in range(half)]
     far = [("f", d) for d in range(half)]
-    while near or far:
-        if far:
-            order.append(far.pop(0))
-        if near and (len(order) > 2 or not far):
-            order.append(near.pop(0))
-    return order
+    early = half // 2
+    return near[:1] + far[:early] + near[1:] + far[early:]
 
 
 def padded(rows):
@@ -350,8 +345,11 @@
         return dict(
             mx=((rows, width), bf),
             wq=((width, 4 * HEAD), bf),
-            wk1=((width, HEAD), bf),
-            wk2=((width, HEAD), bf),
+            wk=((2 * HEAD, width), bf),
+            x=((tokens, width), bf),
+            info=((8, tokens), f32),
+            ids=((2, tokens), jnp.int32),
+            gates=((2, tokens), f32),
             wv=((width, vd), bf),
             wo=((2 * vd, width), bf),
             wg=((width, hidden), bf),
@@ -403,17 +401,54 @@
         return total
 
 
+def step_plan(half):
+    early = half // 2
+    plan = {0: []}
+    late = half - 1
+    for d in range(early):
+        plan[1 + d] = [("crossed", d), ("core_sum", "n", 0) if d == 0 else ("core_sum", "f", d - 1)]
+    first = 1 + early
+    for d in range(1, half):
+        actions = [("arrive_near", d)]
+        if d == 1:
+            actions += [("core_sum", "f", early - 1), ("relay_kv",)]
+        else:
+            actions += [("core_sum", "n", d - 1)]
+            if d - 2 < early:
+                actions += [("side_sum", d - 2)]
+        plan[first + d - 1] = actions
+    for d in range(early, half):
+        actions = [("arrive_far", d)]
+        if d == early:
+            actions += [("core_sum", "n", half - 1)]
+            actions += [("side_sum", e) for e in range(max(half - 2, 0), early)]
+            actions += [("kv_arrivals",), ("head", 0), ("head", 1)]
+        else:
+            actions += [("core_sum", "f", d - 1)]
+        if d == late:
+            actions += [("project_out",)]
+        actions += [("crossed", d)]
+        plan[first + late + d - early] = actions
+    last = 2 * half
+    plan[last] = [("core_sum", "f", half - 1)]
+    plan[last] += [("side_sum", d) for d in range(early, half - 1)]
+    plan[last] += [("mix_sum",), ("other_rows",), ("side_sum", half - 1), ("own_rows",)]
+    return plan
+
+
 class Later:
     def __init__(self, start):
         self.start = start
 
 
 def fused_kernel(sizes, keys, *refs):
-    (lam, info, x, xgain, mgain, hgain) = refs[:6]
-    (h_mx, h_q1, h_q2, h_k1, h_k2, h_v, h_wo, h_g, h_u, h_d, h_sg, h_su, h_sd) = refs[6:19]
-    mix_out, exp_out = refs[19:21]
-    b = dict(zip(keys, refs[21 : 21 + len(keys)]))
-    send_sem, recv_sem, load_sem = refs[21 + len(keys) :]
+    lam, xgain, mgain, hgain = refs[:4]
+    (h_x, h_ids, h_gates, h_mx, h_q1, h_q2, h_k1, h_k2, h_v) = refs[4:13]
+    (h_wo, h_g, h_u, h_d, h_sg, h_su, h_sd) = refs[13:20]
+    mix_out, exp_out = refs[20:22]
+    b = dict(zip(keys, refs[22 : 22 + len(keys)]))
+    send_sem, recv_sem, load_sem = refs[22 + len(keys) :]
+    x, info = b["x"], b["info"]
     half, ep, width, stride, cap = sizes.half, sizes.ep, sizes.width, sizes.stride, sizes.cap
     tokens, rows, tile, vd = sizes.tokens, sizes.rows, sizes.tile, sizes.value_dim
     f32, bf = jnp.float32, jnp.bfloat16
@@ -433,6 +468,7 @@
     near_by = [side * half + (spot + half - d) % half for d in range(half)]
     far_to = [(1 - side) * half + (spot + d) % half for d in range(half)]
     far_by = [(1 - side) * half + (spot + half - d) % half for d in range(half)]
+    early = half // 2
 
     def near(d):
         return (near_to[d], tp)
@@ -472,13 +508,36 @@
     def dot(left, right):
         return jnp.dot(left, right, preferred_element_type=f32)
 
+    for d in range(half):
+        position = place[("f", d)]
+        copies[("FY", d)] = (
+            lambda position=position: b["r"].at[position, 0, 0, pl.ds(0, cap)],
+            lambda position=position: b["r"].at[position, 0, 1, pl.ds(0, cap)],
+            partner_y,
+        )
+        copies[("FRET", d)] = (
+            lambda position=position: b["fb"].at[position, pl.ds(0, cap)],
+            lambda d=d: b["tf"].at[d, pl.ds(0, cap)],
+            far_from(d),
+        )
+    for d in range(1, half):
+        position = place[("n", d)]
+        copies[("NRET", d)] = (
+            lambda position=position: b["q"].at[position, :, pl.ds(0, cap)],
+            lambda d=d: b["tn"].at[:, d, pl.ds(0, cap)],
+            near_from(d),
+        )
+
     loads = {}
     pairs = dict(
+        x=(h_x, b["x"]),
+        ids=(h_ids, b["ids"]),
+        gates=(h_gates, b["gates"]),
         mx=(h_mx, b["mx"]),
         q1=(h_q1, b["wq"].at[:, : 2 * HEAD]),
         q2=(h_q2, b["wq"].at[:, 2 * HEAD :]),
-        k1=(h_k1, b["wk1"]),
-        k2=(h_k2, b["wk2"]),
+        k1=(h_k1, b["wk"].at[:HEAD]),
+        k2=(h_k2, b["wk"].at[HEAD:]),
         v=(h_v, b["wv"]),
         sg=(h_sg, b["sg"]),
         su=(h_su, b["su"]),
@@ -510,7 +569,13 @@
             factor = lax.rsqrt(jnp.mean(values * values, axis=-1, keepdims=True) + EPS)
             target[at, :] = (values * factor * gain[...]).astype(bf)
 
+    loads["x"].wait()
     norm_rows(x, b["xb"].at[0, 0], tokens, xgain)
+    loads["ids"].wait()
+    loads["gates"].wait()
+    info[...] = jnp.zeros((8, tokens), f32)
+    info[0:2, :] = b["ids"][...].astype(f32)
+    info[2:4, :] = b["gates"][...]
 
     earlier = (
         lax.broadcasted_iota(jnp.int32, (tokens, tokens), 0)
@@ -600,7 +665,7 @@
             far(d),
         ).start()
 
-    for d in range(half // 2):
+    for d in range(early):
         start_far(d)
 
     loads["mx"].wait()
@@ -608,8 +673,9 @@
     for name in ("q1", "q2", "k1", "k2", "v"):
         loads[name].wait()
     lane = lax.broadcasted_iota(jnp.int32, (rows, 2 * HEAD), 1)
-    b["kv"][me, :, 0:HEAD] = dot(b["nm"][...], b["wk1"][...]).astype(bf)
-    b["kv"][me, :, HEAD : 2 * HEAD] = dot(b["nm"][...], b["wk2"][...]).astype(bf)
+    b["kv"][me, :, : 2 * HEAD] = lax.dot_general(
+        b["nm"][...], b["wk"][...], (((1,), (1,)), ((), ())), preferred_element_type=f32
+    ).astype(bf)
     b["kv"][me, :, 2 * HEAD :] = dot(b["nm"][...], b["wv"][...]).astype(bf)
 
     copy(("KVF", 0), lambda: b["kv"].at[me], lambda: b["kv"].at[me], far(0))
@@ -624,9 +690,6 @@
         @pl.when(near_to[d] > me)
         def _(d=d):
             made(("KVN", d)).start()
-
-    for d in range(half // 2, half):
-        start_far(d)
 
     for m in range(2):
         queries = dot(b["nm"][...], b["wq"][:, m * 2 * HEAD : (m + 1) * 2 * HEAD])
@@ -659,6 +722,8 @@
     other_place, other_weight = routing(b["other"])
     pick(select(other_place, near_set), b["xb"].at[1, 0], store_near(1))
     start_near(1)
+    for d in range(early, half):
+        start_far(d)
     b["r"][0, 0] = b["outn"][0]
 
     def core_forward(position):
@@ -667,6 +732,9 @@
         )
 
     core_forward(0).start()
+    for d in range(early):
+        made(("FAR", d)).wait_recv()
+        made(("FY", d)).start()
     for which, (at, wt, group) in enumerate(
         ((own_place, own_weight, near_set), (own_place, own_weight, far_set))
     ):
@@ -713,30 +781,6 @@
             def _(d=d):
                 made(("KVC", d)).start()
 
-    events = {}
-
-    def at_step(step, action):
-        events.setdefault(max(step, 0), []).append(action)
-
-    for position, (kind, d) in enumerate(order):
-        if kind == "f":
-            copies[("FY", d)] = (
-                lambda position=position: b["r"].at[position, 0, 0, pl.ds(0, cap)],
-                lambda position=position: b["r"].at[position, 0, 1, pl.ds(0, cap)],
-                partner_y,
-            )
-            at_step(position - 2, functools.partial(arrive_far, d))
-            at_step(position - 1, functools.partial(crossed, d))
-        elif d > 0:
-            at_step(position - 1, functools.partial(arrive_near, d))
-    at_step(3, relay_kv)
-
-    def is_one(value, choices):
-        found = value == choices[0]
-        for choice in choices[1:]:
-            found = jnp.logical_or(found, value == choice)
-        return found
-
     far_places = [place[("f", d)] for d in range(half)]
     row_count = 4 * stride
 
@@ -753,98 +797,43 @@
             partner_y,
         )
 
-    def step_body(step, carry):
-        for when, actions in sorted(events.items()):
-
-            @pl.when(step == when)
-            def _(actions=actions):
-                for action in actions:
-                    action()
-
-        @pl.when(step < ep)
-        def _():
-            core_forward(step).wait_recv()
-            arrived = b["r"][step].reshape(row_count, width)
-            gated = dot(arrived, b["wg"][...])
-            lifted = dot(arrived, b["wu"][...])
-            hidden = (jax.nn.silu(gated) * lifted).astype(bf)
-
-            for n in range(tiles):
-                cols = slice(n * tile, (n + 1) * tile)
-                part = dot(hidden, b["wd"][:, cols]).astype(bf)
-                b["p"][step, :, :, :, cols] = part.reshape(2, 2, stride, tile)
-            back_copy(step).start()
-
-        last = step - 1
-
-        @pl.when(jnp.logical_and(last >= 0, last < ep))
-        def _():
-            back_copy(last).wait_recv()
+    def core_sum(kind, d):
+        position = place[(kind, d)]
+        back_copy(position).wait_recv()
+        for a in range(2):
+            b["q"][position, a] = (
+                b["p"][position, 0, a].astype(f32) + b["pr"][position, a].astype(f32)
+            ).astype(bf)
+        if kind == "f":
+            cross_copy(position).start()
+        elif d > 0:
+            made(("NRET", d)).start()
+        else:
             for a in range(2):
-                b["q"][last, a] = (
-                    b["p"][last, 0, a].astype(f32) + b["pr"][last, a].astype(f32)
-                ).astype(bf)
-
-            @pl.when(last == 0)
-            def _():
-                for a in range(2):
-                    b["tn"][a, 0, 0:cap, :] = b["q"][0, a, 0:cap, :]
-
-            for d in range(1, half):
-                at = place[("n", d)]
-                copy(
-                    ("NRET", d),
-                    lambda at=at: b["q"].at[at, :, pl.ds(0, cap)],
-                    lambda d=d: b["tn"].at[:, d, pl.ds(0, cap)],
-                    near_from(d),
-                )
-
-                @pl.when(last == at)
-                def _(d=d):
-                    made(("NRET", d)).start()
-
-            @pl.when(is_one(last, far_places))
-            def _():
-                cross_copy(last).start()
-
-        older = step - 2
-
-        @pl.when(jnp.logical_and(older >= 0, is_one(older, far_places)))
-        def _():
-            cross_copy(older).wait_recv()
-            b["fb"][older] = (
-                b["q"][older, 0].astype(f32) + b["qr"][older].astype(f32)
-            ).astype(bf)
-            for d in range(half):
-                at = place[("f", d)]
-                copy(
-                    ("FRET", d),
-                    lambda at=at: b["fb"].at[at, pl.ds(0, cap)],
-                    lambda d=d: b["tf"].at[d, pl.ds(0, cap)],
-                    far_from(d),
-                )
-
-                @pl.when(older == at)
-                def _(d=d):
-                    made(("FRET", d)).start()
-
-        return carry
-
-    lax.fori_loop(0, ep + 2, step_body, 0)
+                b["tn"][a, 0, 0:cap, :] = b["q"][position, a, 0:cap, :]
+
+    def side_sum(d):
+        position = place[("f", d)]
+        cross_copy(position).wait_recv()
+        b["fb"][position] = (
+            b["q"][position, 0].astype(f32) + b["qr"][position].astype(f32)
+        ).astype(bf)
+        made(("FRET", d)).start()
 
     def kv_arrival(name, source, d):
         block = b["kv"].at[source]
         remote(table[(name, d)], block, block, near(d)).wait_recv()
 
-    for d in range(1, half):
-
-        @pl.when(near_by[d] < me)
-        def _(d=d):
-            kv_arrival("KVN", near_by[d], d)
-
-        @pl.when(side == 1)
-        def _(d=d):
-            kv_arrival("KVC", (1 - side) * half + (spot + half - d) % half, d)
+    def kv_arrivals():
+        for d in range(1, half):
+
+            @pl.when(near_by[d] < me)
+            def _(d=d):
+                kv_arrival("KVN", near_by[d], d)
+
+            @pl.when(side == 1)
+            def _(d=d):
+                kv_arrival("KVC", (1 - side) * half + (spot + half - d) % half, d)
 
     scale = HEAD**-0.5 * math.log2(math.e)
     row_place = me * rows + lax.broadcasted_iota(jnp.int32, (rows, rows), 0)
@@ -895,41 +884,87 @@
         factor = lax.rsqrt(jnp.mean(combined * combined, axis=1, keepdims=True) + EPS)
         b["hr"][:, g * vd : (g + 1) * vd] = (combined * factor * hgain[...]).astype(bf)
 
-    for g in range(2):
-        head(g)
-
-    loads["wo"].wait()
-    own = sizes.own
-    for n in range(tiles):
-        cols = slice(n * tile, (n + 1) * tile)
-        part = dot(b["hr"][...], b["wo"][:, cols]).astype(bf)
-        b["o"][:, :, :, cols] = part.reshape(2, 2, own, tile)
-    copy(("OC", 0), lambda: b["o"].at[:, 1 - core], lambda: b["orx"], partner_c).start()
-
-    for d in range(1, half):
-        made(("NRET", d)).wait_recv()
-    for a in range(2):
-        made(("SC", a)).wait_recv()
-    for n in range(tiles):
-        cols = slice(n * tile, (n + 1) * tile)
-        back = b["tn"][1, :, :, cols].reshape(half * stride, tile)
-        total = dot(b["woth"][0], back) + dot(b["woth"][1], back)
-        total = total + b["s"][1, 0, :, cols].astype(f32) + b["sr"][1, :, cols].astype(f32)
-        b["ao"][:, cols] = total.astype(bf)
-    copy(("AY", 0), lambda: b["ao"], lambda: b["ar"], partner_y).start()
-
-    made(("OC", 0)).wait_recv()
-    for a in range(2):
-        b["oq"][a] = (b["o"][a, core].astype(f32) + b["orx"][a].astype(f32)).astype(bf)
-    copy(("OY", 0), lambda: b["oq"].at[1 - row_of], lambda: b["oy"], partner_y).start()
-
-    for n in range(tiles):
-        cols = slice(n * tile, (n + 1) * tile)
-        back = b["tn"][0, :, :, cols].reshape(half * stride, tile)
-        total = dot(b["wown"][0, 0], back) + dot(b["wown"][0, 1], back)
-        b["acc"][:, cols] = (
-            total + b["s"][0, 0, :, cols].astype(f32) + b["sr"][0, :, cols].astype(f32)
-        )
+    def project_out():
+        loads["wo"].wait()
+        own = sizes.own
+        for n in range(tiles):
+            cols = slice(n * tile, (n + 1) * tile)
+            part = dot(b["hr"][...], b["wo"][:, cols]).astype(bf)
+            b["o"][:, :, :, cols] = part.reshape(2, 2, own, tile)
+        made(("OC", 0)).start()
+
+    def other_rows():
+        for d in range(1, half):
+            made(("NRET", d)).wait_recv()
+        for a in range(2):
+            made(("SC", a)).wait_recv()
+        for n in range(tiles):
+            cols = slice(n * tile, (n + 1) * tile)
+            back = b["tn"][1, :, :, cols].reshape(half * stride, tile)
+            total = dot(b["woth"][0], back) + dot(b["woth"][1], back)
+            total = total + b["s"][1, 0, :, cols].astype(f32) + b["sr"][1, :, cols].astype(f32)
+            b["ao"][:, cols] = total.astype(bf)
+        made(("AY", 0)).start()
+
+    def mix_sum():
+        made(("OC", 0)).wait_recv()
+        for a in range(2):
+            b["oq"][a] = (b["o"][a, core].astype(f32) + b["orx"][a].astype(f32)).astype(bf)
+        made(("OY", 0)).start()
+
+    def own_rows():
+        for n in range(tiles):
+            cols = slice(n * tile, (n + 1) * tile)
+            back = b["tn"][0, :, :, cols].reshape(half * stride, tile)
+            total = dot(b["wown"][0, 0], back) + dot(b["wown"][0, 1], back)
+            b["acc"][:, cols] = (
+                total + b["s"][0, 0, :, cols].astype(f32) + b["sr"][0, :, cols].astype(f32)
+            )
+
+    copies[("OC", 0)] = (lambda: b["o"].at[:, 1 - core], lambda: b["orx"], partner_c)
+    copies[("AY", 0)] = (lambda: b["ao"], lambda: b["ar"], partner_y)
+    copies[("OY", 0)] = (lambda: b["oq"].at[1 - row_of], lambda: b["oy"], partner_y)
+    schedule = step_plan(half)
+    actions = dict(
+        arrive_far=arrive_far,
+        crossed=crossed,
+        arrive_near=arrive_near,
+        core_sum=core_sum,
+        side_sum=side_sum,
+        relay_kv=relay_kv,
+        kv_arrivals=kv_arrivals,
+        head=head,
+        project_out=project_out,
+        mix_sum=mix_sum,
+        other_rows=other_rows,
+        own_rows=own_rows,
+    )
+
+    def step_body(step, carry):
+        for when in sorted(schedule):
+
+            @pl.when(step == when)
+            def _(when=when):
+                for name, *values in schedule[when]:
+                    actions[name](*values)
+
+        @pl.when(step < ep)
+        def _():
+            core_forward(step).wait_recv()
+            arrived = b["r"][step].reshape(row_count, width)
+            gated = dot(arrived, b["wg"][...])
+            lifted = dot(arrived, b["wu"][...])
+            hidden = (jax.nn.silu(gated) * lifted).astype(bf)
+            for n in range(tiles):
+                cols = slice(n * tile, (n + 1) * tile)
+                part = dot(hidden, b["wd"][:, cols]).astype(bf)
+                b["p"][step, :, :, :, cols] = part.reshape(2, 2, stride, tile)
+            back_copy(step).start()
+
+        return carry
+
+    lax.fori_loop(0, max(schedule) + 1, step_body, 0)
+
     made(("OY", 0)).wait_recv()
     mix_out[...] = (b["oq"][row_of].astype(f32) + b["oy"][...].astype(f32)).astype(bf)
 
@@ -976,13 +1011,13 @@
             jax.ShapeDtypeStruct((sizes.own, sizes.width), jnp.bfloat16),
             jax.ShapeDtypeStruct((sizes.tokens, sizes.width), jnp.bfloat16),
         ),
-        in_specs=[smem] + [vmem] * 5 + [hbm] * 13,
+        in_specs=[smem] + [vmem] * 3 + [hbm] * 16,
         out_specs=(vmem, vmem),
         scratch_shapes=[pltpu.VMEM(shape, dtype) for shape, dtype in scratch.values()]
         + [
             pltpu.SemaphoreType.DMA((count,)),
             pltpu.SemaphoreType.DMA((count,)),
-            pltpu.SemaphoreType.DMA((13,)),
+            pltpu.SemaphoreType.DMA((16,)),
         ],
         compiler_params=pltpu.CompilerParams(
             collective_id=0, has_side_effects=True, vmem_limit_bytes=VMEM_LIMIT
@@ -1017,28 +1052,21 @@
         shared_up,
         shared_down,
     ) = arrays
-    info = jnp.concatenate(
-        [
-            routes.T.astype(jnp.float32),
-            route_weight.T,
-            jnp.zeros((4, sizes.tokens), jnp.float32),
-        ],
-        axis=0,
-    )
     return fused(
         sizes,
         (
             lambdas,
-            info,
-            expert_input,
             expert_gain.reshape(1, -1),
             mixer_gain.reshape(1, -1),
             head_gain.reshape(1, -1),
+            expert_input,
+            routes.T,
+            route_weight.T,
             mixer_input,
             query_one,
             query_two,
-            key_one,
-            key_two,
+            key_one.T,
+            key_two.T,
             value_weight,
             output_weight,
             expert_gate,

time: 111 us -> 101 us (0.910)
  the two profiles are of different devices: /device:TPU:0 before, /device:TPU:31 now
where the time goes in v2:
time: 101 us
  Pallas kernels  97.9 us (97%)
  local copies, waits for them, and re-layouts  2.52 us (2%)
    pallas_call x1, Pallas kernels, fused(): pl.pallas_call(functools.partial(fused_kernel, sizes, keys), out_shape=(j...  97.9 us
    unnamed x4, local copies, waits for them, and re-layouts  2.52 us

profile of v2, /device:TPU:31, one launch (start us, length us, event | category | flops | bytes accessed | tf_op | source)
XLA Modules:
  0.0 101.1 jit_solution(2141120154112903383)
XLA Ops:
  0.6 97.9 %layer.1 = (bf16[64,2048]{1,0:T(8,128)(2,1)}, bf16[128,2048]{1,0:T(8,128)(2,1)}) custom-call(f32[2]{0:T(128)} %refs_0_.1, f32[1,2048]{1,0:T(1,128)} %bitcast.9, f32[1,2048]{1,0:T(1,128)} %bitcast.10, f32[1,128]{1,0:T(1,128)} %bitcast.13, bf16[128,2048]{1,0:T(8,128)(2,1)} %refs_4_.1, s32[2,128]{1,0:T(2,128)} %bitcast.11, f32[2,128]{1,0:T(2,128)} %bitcast.12, ...), custom_call_target="tpu_custom_call" | custom-call | tf_op jit(solution)/shard_map/layer/pallas_call | solution.py:1008
  98.6 0.0 copy-start
  98.6 1.7 %copy.24 = bf16[64,2048]{1,0:T(8,128)(2,1)} copy(bf16[64,2048]{1,0:T(8,128)(2,1)} %get-tuple-element.4) | data formatting | bytes 524288
  100.3 0.0 copy-done
  100.3 0.8 copy.25
Async XLA Ops:
  98.6 1.7 %copy-start = (bf16[128,2048]{1,0:T(8,128)(2,1)S(1)}, bf16[128,2048]{1,0:T(8,128)(2,1)}, u32[]{:S(2)}) copy-start(bf16[128,2048]{1,0:T(8,128)(2,1)} %get-tuple-element.5) | copy-start | bytes 1572868

commit v3 on v2

--- a/solution.py
+++ b/solution.py
@@ -299,10 +299,9 @@
 
 
 def chunk_order(half):
-    near = [("n", d) for d in range(half)]
-    far = [("f", d) for d in range(half)]
-    early = half // 2
-    return near[:1] + far[:early] + near[1:] + far[early:]
+    order = [("n", 0)] + [("n", 2)] * (half > 2) + [("n", 1)]
+    order += [("n", d) for d in range(3, half)]
+    return order + [("f", d) for d in range(half)]
 
 
 def padded(rows):
@@ -321,14 +320,16 @@
 
     def names(self):
         half, ep = self.half, self.ep
+        crossing = [("n", d) for d in range(2, half)] + [("f", d) for d in range(half)]
         groups = (
             [("XY", 0), ("INFO", 0), ("XC", 0), ("XC", 1)]
             + [("FAR", d) for d in range(half)]
-            + [("NEAR", d, a) for d in range(1, half) for a in range(2)]
-            + [("FY", d) for d in range(half)]
-            + [("NRET", d) for d in range(1, half)]
-            + [("FRET", d) for d in range(half)]
-            + [("SC", 0), ("SC", 1), ("AY", 0), ("KVF", 0), ("OC", 0), ("OY", 0)]
+            + [("NEAR", d, 0) for d in range(1, half)]
+            + [("NEAR", 1, 1)]
+            + [("FY",) + name for name in crossing]
+            + [("RET", d) for d in range(half)]
+            + [("NRET", d, c) for d in range(1, half) for c in range(2)]
+            + [("SC", 0), ("SC", 1), ("AY", 0), ("AY", 1), ("KVF", 0), ("OC", 0), ("OY", 0)]
             + [("KVN", d) for d in range(1, half)]
             + [("KVC", d) for d in range(1, half)]
         )
@@ -375,7 +376,8 @@
             ao=((tokens, width), bf),
             ar=((tokens, width), bf),
             acc=((tokens, width), f32),
-            wown=((2, 2, tokens, half * stride), bf),
+            wown=((2, tokens, half * stride), bf),
+            wfar=((2, tokens, half * stride), bf),
             woth=((2, tokens, half * stride), bf),
             nm=((rows, width), bf),
             qs=((2, 2, rows, 2 * HEAD), bf),
@@ -402,37 +404,35 @@
 
 
 def step_plan(half):
+    order = chunk_order(half)
+    place = {name: number for number, name in enumerate(order)}
+    plan = {number: [] for number in range(2 * half + 1)}
     early = half // 2
-    plan = {0: []}
-    late = half - 1
+    plan[place[("n", 1)]] += [("core_sum", "n", 0), ("arrive_near",)]
+    for d in range(2, half):
+        plan[place[("n", d)]] += [("crossed", "n", d)]
     for d in range(early):
-        plan[1 + d] = [("crossed", d), ("core_sum", "n", 0) if d == 0 else ("core_sum", "f", d - 1)]
-    first = 1 + early
+        plan[place[("f", d)] - 1] += [("crossed", "f", d)]
     for d in range(1, half):
-        actions = [("arrive_near", d)]
-        if d == 1:
-            actions += [("core_sum", "f", early - 1), ("relay_kv",)]
-        else:
-            actions += [("core_sum", "n", d - 1)]
-            if d - 2 < early:
-                actions += [("side_sum", d - 2)]
-        plan[first + d - 1] = actions
+        plan[place[("n", d)] + 2] += [("core_sum", "n", d)]
+    for d in range(early):
+        plan[place[("f", d)] + 2] += [("core_sum", "f", d)]
     for d in range(early, half):
-        actions = [("arrive_far", d)]
-        if d == early:
-            actions += [("core_sum", "n", half - 1)]
-            actions += [("side_sum", e) for e in range(max(half - 2, 0), early)]
-            actions += [("kv_arrivals",), ("head", 0), ("head", 1)]
-        else:
-            actions += [("core_sum", "f", d - 1)]
-        if d == late:
-            actions += [("project_out",)]
-        actions += [("crossed", d)]
-        plan[first + late + d - early] = actions
-    last = 2 * half
-    plan[last] = [("core_sum", "f", half - 1)]
-    plan[last] += [("side_sum", d) for d in range(early, half - 1)]
-    plan[last] += [("mix_sum",), ("other_rows",), ("side_sum", half - 1), ("own_rows",)]
+        plan[place[("f", d)] - 1] += [("arrive_cross", "f", d)]
+    first = plan[place[("f", early)]]
+    first += [("kv_arrivals",), ("head", 0), ("crossed", "f", early)]
+    for d in range(early + 1, half):
+        now = plan[place[("f", d)]]
+        now += [("side_sum", d - early - 1)]
+        if d == early + 1:
+            now += [("head", 1), ("project_out",)]
+        now += [("crossed", "f", d)]
+    last = plan[2 * half]
+    last += [("core_sum", "f", d) for d in range(early, half - 1)]
+    last += [("side_sum", d) for d in range(half - early - 1, early)]
+    last += [("core_sum", "f", half - 1), ("mix_sum",)]
+    last += [("side_sum", d) for d in range(early, half)]
+    last += [("other_rows", 0), ("other_rows", 1), ("own_rows",)]
     return plan
 
 
@@ -464,10 +464,17 @@
     core = tp % 2
     tiles = width // tile
 
-    near_to = [side * half + (spot + d) % half for d in range(half)]
-    near_by = [side * half + (spot + half - d) % half for d in range(half)]
-    far_to = [(1 - side) * half + (spot + d) % half for d in range(half)]
-    far_by = [(1 - side) * half + (spot + half - d) % half for d in range(half)]
+    lines = half // 2
+    line, lane_x = spot // 2, spot % 2
+
+    def shifted(which, d, turn):
+        moved = (line + lines + turn * (d // 2)) % lines
+        return which * half + moved * 2 + (lane_x + d % 2) % 2
+
+    near_to = [shifted(side, d, 1) for d in range(half)]
+    near_by = [shifted(side, d, -1) for d in range(half)]
+    far_to = [shifted(1 - side, d, 1) for d in range(half)]
+    far_by = [shifted(1 - side, d, -1) for d in range(half)]
     early = half // 2
 
     def near(d):
@@ -508,25 +515,28 @@
     def dot(left, right):
         return jnp.dot(left, right, preferred_element_type=f32)
 
-    for d in range(half):
-        position = place[("f", d)]
-        copies[("FY", d)] = (
+    crossing = [("n", d) for d in range(2, half)] + [("f", d) for d in range(half)]
+    for kind, d in crossing:
+        position = place[(kind, d)]
+        copies[("FY", kind, d)] = (
             lambda position=position: b["r"].at[position, 0, 0, pl.ds(0, cap)],
             lambda position=position: b["r"].at[position, 0, 1, pl.ds(0, cap)],
             partner_y,
         )
-        copies[("FRET", d)] = (
-            lambda position=position: b["fb"].at[position, pl.ds(0, cap)],
+    for d in range(half):
+        copies[("RET", d)] = (
+            lambda d=d: b["fb"].at[place[("f", d)], pl.ds(0, cap)],
             lambda d=d: b["tf"].at[d, pl.ds(0, cap)],
             far_from(d),
         )
     for d in range(1, half):
-        position = place[("n", d)]
-        copies[("NRET", d)] = (
-            lambda position=position: b["q"].at[position, :, pl.ds(0, cap)],
-            lambda d=d: b["tn"].at[:, d, pl.ds(0, cap)],
-            near_from(d),
-        )
+        for c in range(2):
+            cols = pl.ds(c * width // 2, width // 2)
+            copies[("NRET", d, c)] = (
+                lambda d=d, cols=cols: b["q"].at[place[("n", d)], :, pl.ds(0, cap), cols],
+                lambda d=d, cols=cols: b["tn"].at[:, d, pl.ds(0, cap), cols],
+                near_from(d),
+            )
 
     loads = {}
     pairs = dict(
@@ -583,11 +593,9 @@
     ).astype(bf)
     padded_ep = -(-ep // 8) * 8
     relative = lax.broadcasted_iota(jnp.int32, (padded_ep, tokens), 0)
-    in_far = relative >= half
-    turn = jnp.where(in_far, relative - half, relative) + spot
-    turn = jnp.where(turn >= half, turn - half, turn)
-    names_half = jnp.where(in_far, 1 - side, side)
-    expert = (names_half * half + turn).astype(f32)
+    expert = jnp.zeros((padded_ep, tokens), f32) - 1.0
+    for k, target in enumerate(near_to + far_to):
+        expert = jnp.where(relative == k, target.astype(f32), expert)
 
     def routing(info_ref):
         first = info_ref[0:1, :] == expert
@@ -619,6 +627,7 @@
     own_place, own_weight = routing(info)
     near_set = list(range(half))
     far_set = list(range(half, 2 * half))
+    direct_set = [0, 1]
     select_near = select(own_place, near_set)
     select_far = select(own_place, far_set)
 
@@ -631,7 +640,7 @@
         for n in range(tiles):
             cols = slice(n * tile, (n + 1) * tile)
             picked = dot(select_rows, source[:, cols]).astype(bf)
-            for d in range(half):
+            for d in range(select_rows.shape[0] // stride):
                 store(d, cols, picked[d * stride : (d + 1) * stride, :])
 
     def store_near(a):
@@ -645,8 +654,44 @@
 
     pick(select_near, b["xb"].at[0, 0], store_near(0))
 
+    def core_forward(position):
+        return remote(
+            table["RC"] + position, b["r"].at[position, 0], b["r"].at[position, 1], partner_c
+        )
+
+    def arrive_cross(kind, d):
+        made(("FAR", d) if kind == "f" else ("NEAR", d, 0)).wait_recv()
+        made(("FY", kind, d)).start()
+
+    def crossed(kind, d):
+        made(("FY", kind, d)).wait_recv()
+        core_forward(place[(kind, d)]).start()
+
+    def arrive_near():
+        for a in range(2):
+            made(("NEAR", 1, a)).wait_recv()
+        core_forward(place[("n", 1)]).start()
+
+    def relay_kv():
+        @pl.when(side == 1)
+        def _():
+            slot_of = b["kv"].at[far_by[0]]
+            remote(table[("KVF", 0)], slot_of, slot_of, far(0)).wait_recv()
+
+        for d in range(1, half):
+            copy(("KVC", d), lambda: b["kv"].at[far_by[0]], lambda: b["kv"].at[far_by[0]], near(d))
+
+            @pl.when(side == 1)
+            def _(d=d):
+                made(("KVC", d)).start()
+
+    def other_spread():
+        upper, lower = spread(other_place, other_weight, near_set)
+        b["woth"][0] = upper
+        b["woth"][1] = lower
+
     def start_near(a):
-        for d in range(1, half):
+        for d in (range(1, half) if a == 0 else (1,)):
             copy(
                 ("NEAR", d, a),
                 lambda d=d: b["outn"].at[d, a, pl.ds(0, cap)],
@@ -665,8 +710,7 @@
             far(d),
         ).start()
 
-    for d in range(early):
-        start_far(d)
+    start_far(0)
 
     loads["mx"].wait()
     norm_rows(b["mx"], b["nm"], rows, mgain)
@@ -690,6 +734,9 @@
         @pl.when(near_to[d] > me)
         def _(d=d):
             made(("KVN", d)).start()
+
+    for d in range(1, early):
+        start_far(d)
 
     for m in range(2):
         queries = dot(b["nm"][...], b["wq"][:, m * 2 * HEAD : (m + 1) * 2 * HEAD])
@@ -716,70 +763,38 @@
     shared_expert(0)
     copy(("SC", 0), lambda: b["s"].at[0, 1], lambda: b["sr"].at[0], partner_c).start()
 
+    for name, group in (("wown", near_set), ("wfar", far_set)):
+        upper, lower = spread(own_place, own_weight, group)
+        b[name][0] = upper
+        b[name][1] = lower
+    for d in range(half):
+        b["tf"][d, cap:, :] = jnp.zeros((stride - cap, width), bf)
+        for a in range(2):
+            b["tn"][a, d, cap:, :] = jnp.zeros((stride - cap, width), bf)
     made(("XY", 0)).wait_recv()
     made(("INFO", 0)).wait_recv()
     copy(("XC", 1), lambda: b["xb"].at[1, 0], lambda: b["xb"].at[1, 1], partner_c).start()
+    for d in range(2, half):
+        arrive_cross("n", d)
     other_place, other_weight = routing(b["other"])
-    pick(select(other_place, near_set), b["xb"].at[1, 0], store_near(1))
+    pick(select(other_place, direct_set), b["xb"].at[1, 0], store_near(1))
+    relay_kv()
     start_near(1)
     for d in range(early, half):
         start_far(d)
     b["r"][0, 0] = b["outn"][0]
 
-    def core_forward(position):
-        return remote(
-            table["RC"] + position, b["r"].at[position, 0], b["r"].at[position, 1], partner_c
-        )
-
     core_forward(0).start()
-    for d in range(early):
-        made(("FAR", d)).wait_recv()
-        made(("FY", d)).start()
-    for which, (at, wt, group) in enumerate(
-        ((own_place, own_weight, near_set), (own_place, own_weight, far_set))
-    ):
-        upper, lower = spread(at, wt, group)
-        b["wown"][which, 0] = upper
-        b["wown"][which, 1] = lower
-    upper, lower = spread(other_place, other_weight, near_set)
-    b["woth"][0] = upper
-    b["woth"][1] = lower
-    for d in range(half):
-        b["tf"][d, cap:, :] = jnp.zeros((stride - cap, width), bf)
-        for a in range(2):
-            b["tn"][a, d, cap:, :] = jnp.zeros((stride - cap, width), bf)
+    arrive_cross("f", 0)
     made(("XC", 1)).wait_recv()
     shared_expert(1)
     copy(("SC", 1), lambda: b["s"].at[1, 1], lambda: b["sr"].at[1], partner_c).start()
+    other_spread()
+    for d in range(1, early):
+        arrive_cross("f", d)
 
     for name in ("wg", "wu", "wd"):
         loads[name].wait()
-
-    def arrive_far(d):
-        made(("FAR", d)).wait_recv()
-        made(("FY", d)).start()
-
-    def crossed(d):
-        made(("FY", d)).wait_recv()
-        core_forward(place[("f", d)]).start()
-
-    def arrive_near(d):
-        for a in range(2):
-            made(("NEAR", d, a)).wait_recv()
-        core_forward(place[("n", d)]).start()
-
-    def relay_kv():
-        @pl.when(side == 1)
-        def _():
-            slot_of = b["kv"].at[far_by[0]]
-            remote(table[("KVF", 0)], slot_of, slot_of, far(0)).wait_recv()
-
-        for d in range(1, half):
-            copy(("KVC", d), lambda: b["kv"].at[far_by[0]], lambda: b["kv"].at[far_by[0]], near(d))
-
-            @pl.when(side == 1)
-            def _(d=d):
-                made(("KVC", d)).start()
 
     far_places = [place[("f", d)] for d in range(half)]
     row_count = 4 * stride
@@ -807,7 +822,8 @@
         if kind == "f":
             cross_copy(position).start()
         elif d > 0:
-            made(("NRET", d)).start()
+            for c in range(2):
+                made(("NRET", d, c)).start()
         else:
             for a in range(2):
                 b["tn"][a, 0, 0:cap, :] = b["q"][position, a, 0:cap, :]
@@ -818,7 +834,7 @@
         b["fb"][position] = (
             b["q"][position, 0].astype(f32) + b["qr"][position].astype(f32)
         ).astype(bf)
-        made(("FRET", d)).start()
+        made(("RET", d)).start()
 
     def kv_arrival(name, source, d):
         block = b["kv"].at[source]
@@ -833,7 +849,7 @@
 
             @pl.when(side == 1)
             def _(d=d):
-                kv_arrival("KVC", (1 - side) * half + (spot + half - d) % half, d)
+                kv_arrival("KVC", far_by[d], d)
 
     scale = HEAD**-0.5 * math.log2(math.e)
     row_place = me * rows + lax.broadcasted_iota(jnp.int32, (rows, rows), 0)
@@ -893,18 +909,19 @@
             b["o"][:, :, :, cols] = part.reshape(2, 2, own, tile)
         made(("OC", 0)).start()
 
-    def other_rows():
+    def other_rows(c):
         for d in range(1, half):
-            made(("NRET", d)).wait_recv()
-        for a in range(2):
-            made(("SC", a)).wait_recv()
-        for n in range(tiles):
+            made(("NRET", d, c)).wait_recv()
+        if c == 0:
+            for a in range(2):
+                made(("SC", a)).wait_recv()
+        for n in range(c * tiles // 2, (c + 1) * tiles // 2):
             cols = slice(n * tile, (n + 1) * tile)
             back = b["tn"][1, :, :, cols].reshape(half * stride, tile)
             total = dot(b["woth"][0], back) + dot(b["woth"][1], back)
             total = total + b["s"][1, 0, :, cols].astype(f32) + b["sr"][1, :, cols].astype(f32)
             b["ao"][:, cols] = total.astype(bf)
-        made(("AY", 0)).start()
+        made(("AY", c)).start()
 
     def mix_sum():
         made(("OC", 0)).wait_recv()
@@ -916,22 +933,27 @@
         for n in range(tiles):
             cols = slice(n * tile, (n + 1) * tile)
             back = b["tn"][0, :, :, cols].reshape(half * stride, tile)
-            total = dot(b["wown"][0, 0], back) + dot(b["wown"][0, 1], back)
+            total = dot(b["wown"][0], back) + dot(b["wown"][1], back)
             b["acc"][:, cols] = (
                 total + b["s"][0, 0, :, cols].astype(f32) + b["sr"][0, :, cols].astype(f32)
             )
 
     copies[("OC", 0)] = (lambda: b["o"].at[:, 1 - core], lambda: b["orx"], partner_c)
-    copies[("AY", 0)] = (lambda: b["ao"], lambda: b["ar"], partner_y)
+    for c in range(2):
+        cols = pl.ds(c * width // 2, width // 2)
+        copies[("AY", c)] = (
+            lambda cols=cols: b["ao"].at[:, cols],
+            lambda cols=cols: b["ar"].at[:, cols],
+            partner_y,
+        )
     copies[("OY", 0)] = (lambda: b["oq"].at[1 - row_of], lambda: b["oy"], partner_y)
     schedule = step_plan(half)
     actions = dict(
-        arrive_far=arrive_far,
+        arrive_cross=arrive_cross,
         crossed=crossed,
         arrive_near=arrive_near,
         core_sum=core_sum,
         side_sum=side_sum,
-        relay_kv=relay_kv,
         kv_arrivals=kv_arrivals,
         head=head,
         project_out=project_out,
@@ -969,12 +991,13 @@
     mix_out[...] = (b["oq"][row_of].astype(f32) + b["oy"][...].astype(f32)).astype(bf)
 
     for d in range(half):
-        made(("FRET", d)).wait_recv()
-    made(("AY", 0)).wait_recv()
+        made(("RET", d)).wait_recv()
+    for c in range(2):
+        made(("AY", c)).wait_recv()
     for n in range(tiles):
         cols = slice(n * tile, (n + 1) * tile)
         back = b["tf"][:, :, cols].reshape(half * stride, tile)
-        total = dot(b["wown"][1, 0], back) + dot(b["wown"][1, 1], back)
+        total = dot(b["wfar"][0], back) + dot(b["wfar"][1], back)
         total = total + b["acc"][:, cols] + b["ar"][:, cols].astype(f32)
         exp_out[:, cols] = total.astype(bf)
 

time: 101 us -> 89.8 us (0.89)
  the two profiles are of different devices: /device:TPU:31 before, /device:TPU:23 now
where the time goes in v3:
time: 89.8 us; the launch traced here: 89.7 us
  Pallas kernels  86.5 us (96%)
  local copies, waits for them, and re-layouts  2.52 us (3%)
    pallas_call x1, Pallas kernels, fused(): pl.pallas_call(functools.partial(fused_kernel, sizes, keys), out_shape=(j...  86.5 us
    unnamed x4, local copies, waits for them, and re-layouts  2.52 us

profile of v3, /device:TPU:23, one launch (start us, length us, event | category | flops | bytes accessed | tf_op | source)
XLA Modules:
  0.0 89.7 jit_solution(4466989583289579674)
XLA Ops:
  0.6 86.5 %layer.1 = (bf16[64,2048]{1,0:T(8,128)(2,1)}, bf16[128,2048]{1,0:T(8,128)(2,1)}) custom-call(f32[2]{0:T(128)} %refs_0_.1, f32[1,2048]{1,0:T(1,128)} %bitcast.9, f32[1,2048]{1,0:T(1,128)} %bitcast.10, f32[1,128]{1,0:T(1,128)} %bitcast.13, bf16[128,2048]{1,0:T(8,128)(2,1)} %refs_4_.1, s32[2,128]{1,0:T(2,128)} %bitcast.11, f32[2,128]{1,0:T(2,128)} %bitcast.12, ...), custom_call_target="tpu_custom_call" | custom-call | tf_op jit(solution)/shard_map/layer/pallas_call | solution.py:1031
  87.1 0.0 copy-start
  87.1 1.7 %copy.24 = bf16[64,2048]{1,0:T(8,128)(2,1)} copy(bf16[64,2048]{1,0:T(8,128)(2,1)} %get-tuple-element.4) | data formatting | bytes 524288
  88.9 0.0 copy-done
  88.9 0.8 copy.25
Async XLA Ops:
  87.1 1.7 %copy-start = (bf16[128,2048]{1,0:T(8,128)(2,1)S(1)}, bf16[128,2048]{1,0:T(8,128)(2,1)}, u32[]{:S(2)}) copy-start(bf16[128,2048]{1,0:T(8,128)(2,1)} %get-tuple-element.5) | copy-start | bytes 1572868

commit v4 on v3

--- a/solution.py
+++ b/solution.py
@@ -299,9 +299,10 @@
 
 
 def chunk_order(half):
-    order = [("n", 0)] + [("n", 2)] * (half > 2) + [("n", 1)]
-    order += [("n", d) for d in range(3, half)]
-    return order + [("f", d) for d in range(half)]
+    early = half // 2
+    order = [("n", 0)] + [("f", d) for d in range(early)]
+    order += [("n", d) for d in range(1, half)]
+    return order + [("f", d) for d in range(early, half)]
 
 
 def padded(rows):
@@ -377,7 +378,7 @@
             ar=((tokens, width), bf),
             acc=((tokens, width), f32),
             wown=((2, tokens, half * stride), bf),
-            wfar=((2, tokens, half * stride), bf),
+            wfar=((half, 2, tokens, stride), bf),
             woth=((2, tokens, half * stride), bf),
             nm=((rows, width), bf),
             qs=((2, 2, rows, 2 * HEAD), bf),
@@ -408,30 +409,31 @@
     place = {name: number for number, name in enumerate(order)}
     plan = {number: [] for number in range(2 * half + 1)}
     early = half // 2
-    plan[place[("n", 1)]] += [("core_sum", "n", 0), ("arrive_near",)]
-    for d in range(2, half):
-        plan[place[("n", d)]] += [("crossed", "n", d)]
     for d in range(early):
-        plan[place[("f", d)] - 1] += [("crossed", "f", d)]
+        plan[place[("f", d)]] += [("crossed", "f", d)]
+    plan[early] += [("core_sum", "n", 0), ("relay_kv",)]
+    first = place[("n", 1)]
+    plan[first] += [("crossed", "n", 2)] * (half > 2) + [("arrive_near",)]
+    for d in range(3, half):
+        plan[place[("n", d)] - 1] += [("crossed", "n", d)]
+    for d in range(early):
+        plan[first + d] += [("core_sum", "f", d)]
     for d in range(1, half):
         plan[place[("n", d)] + 2] += [("core_sum", "n", d)]
-    for d in range(early):
-        plan[place[("f", d)] + 2] += [("core_sum", "f", d)]
     for d in range(early, half):
         plan[place[("f", d)] - 1] += [("arrive_cross", "f", d)]
-    first = plan[place[("f", early)]]
-    first += [("kv_arrivals",), ("head", 0), ("crossed", "f", early)]
-    for d in range(early + 1, half):
-        now = plan[place[("f", d)]]
-        now += [("side_sum", d - early - 1)]
-        if d == early + 1:
-            now += [("head", 1), ("project_out",)]
-        now += [("crossed", "f", d)]
+    for d in range(early):
+        plan[first + d + 2] += [("side_sum", d)]
+    for d in range(early, half):
+        at = plan[place[("f", d)]]
+        if d == half - 1:
+            at += [("kv_arrivals",), ("head", 0)]
+        if d > early:
+            at += [("core_sum", "f", d - 1)]
+        at += [("crossed", "f", d)]
     last = plan[2 * half]
-    last += [("core_sum", "f", d) for d in range(early, half - 1)]
-    last += [("side_sum", d) for d in range(half - early - 1, early)]
-    last += [("core_sum", "f", half - 1), ("mix_sum",)]
-    last += [("side_sum", d) for d in range(early, half)]
+    last += [("core_sum", "f", half - 1), ("side_sum", early), ("head", 1), ("project_out",)]
+    last += [("side_sum", d) for d in range(early + 1, half)] + [("mix_sum",)]
     last += [("other_rows", 0), ("other_rows", 1), ("own_rows",)]
     return plan
 
@@ -710,7 +712,8 @@
             far(d),
         ).start()
 
-    start_far(0)
+    for d in range(early):
+        start_far(d)
 
     loads["mx"].wait()
     norm_rows(b["mx"], b["nm"], rows, mgain)
@@ -734,9 +737,6 @@
         @pl.when(near_to[d] > me)
         def _(d=d):
             made(("KVN", d)).start()
-
-    for d in range(1, early):
-        start_far(d)
 
     for m in range(2):
         queries = dot(b["nm"][...], b["wq"][:, m * 2 * HEAD : (m + 1) * 2 * HEAD])
@@ -763,10 +763,13 @@
     shared_expert(0)
     copy(("SC", 0), lambda: b["s"].at[0, 1], lambda: b["sr"].at[0], partner_c).start()
 
-    for name, group in (("wown", near_set), ("wfar", far_set)):
-        upper, lower = spread(own_place, own_weight, group)
-        b[name][0] = upper
-        b[name][1] = lower
+    upper, lower = spread(own_place, own_weight, near_set)
+    b["wown"][0] = upper
+    b["wown"][1] = lower
+    for d in range(half):
+        upper, lower = spread(own_place, own_weight, [half + d])
+        b["wfar"][d, 0] = upper
+        b["wfar"][d, 1] = lower
     for d in range(half):
         b["tf"][d, cap:, :] = jnp.zeros((stride - cap, width), bf)
         for a in range(2):
@@ -774,24 +777,23 @@
     made(("XY", 0)).wait_recv()
     made(("INFO", 0)).wait_recv()
     copy(("XC", 1), lambda: b["xb"].at[1, 0], lambda: b["xb"].at[1, 1], partner_c).start()
-    for d in range(2, half):
-        arrive_cross("n", d)
+    arrive_cross("f", 0)
     other_place, other_weight = routing(b["other"])
     pick(select(other_place, direct_set), b["xb"].at[1, 0], store_near(1))
-    relay_kv()
     start_near(1)
     for d in range(early, half):
         start_far(d)
     b["r"][0, 0] = b["outn"][0]
 
     core_forward(0).start()
-    arrive_cross("f", 0)
     made(("XC", 1)).wait_recv()
     shared_expert(1)
     copy(("SC", 1), lambda: b["s"].at[1, 1], lambda: b["sr"].at[1], partner_c).start()
     other_spread()
     for d in range(1, early):
         arrive_cross("f", d)
+    for d in range(2, half):
+        arrive_cross("n", d)
 
     for name in ("wg", "wu", "wd"):
         loads[name].wait()
@@ -956,6 +958,7 @@
         side_sum=side_sum,
         kv_arrivals=kv_arrivals,
         head=head,
+        relay_kv=relay_kv,
         project_out=project_out,
         mix_sum=mix_sum,
         other_rows=other_rows,
@@ -992,14 +995,14 @@
 
     for d in range(half):
         made(("RET", d)).wait_recv()
+        for n in range(tiles):
+            cols = slice(n * tile, (n + 1) * tile)
+            back = b["tf"][d, :, cols]
+            b["acc"][:, cols] += dot(b["wfar"][d, 0], back) + dot(b["wfar"][d, 1], back)
     for c in range(2):
         made(("AY", c)).wait_recv()
-    for n in range(tiles):
-        cols = slice(n * tile, (n + 1) * tile)
-        back = b["tf"][:, :, cols].reshape(half * stride, tile)
-        total = dot(b["wfar"][0], back) + dot(b["wfar"][1], back)
-        total = total + b["acc"][:, cols] + b["ar"][:, cols].astype(f32)
-        exp_out[:, cols] = total.astype(bf)
+        cols = slice(c * width // 2, (c + 1) * width // 2)
+        exp_out[:, cols] = (b["acc"][:, cols] + b["ar"][:, cols].astype(f32)).astype(bf)
 
     conditional = {("KVF", 0): side == 0}
     for d in range(1, half):

time: 89.8 us -> 86.8 us (0.967)
  the two profiles are of different devices: /device:TPU:23 before, /device:TPU:31 now
where the time goes in v4:
time: 86.8 us; the launch traced here: 85.2 us
  Pallas kernels  82 us (94%)
  local copies, waits for them, and re-layouts  2.52 us (3%)
    pallas_call x1, Pallas kernels, fused(): pl.pallas_call(functools.partial(fused_kernel, sizes, keys), out_shape=(j...  82 us
    unnamed x4, local copies, waits for them, and re-layouts  2.52 us

profile of v4, /device:TPU:31, one launch (start us, length us, event | category | flops | bytes accessed | tf_op | source)
XLA Modules:
  0.0 85.2 jit_solution(14186094259854772681)
XLA Ops:
  0.6 82.0 %layer.1 = (bf16[64,2048]{1,0:T(8,128)(2,1)}, bf16[128,2048]{1,0:T(8,128)(2,1)}) custom-call(f32[2]{0:T(128)} %refs_0_.1, f32[1,2048]{1,0:T(1,128)} %bitcast.9, f32[1,2048]{1,0:T(1,128)} %bitcast.10, f32[1,128]{1,0:T(1,128)} %bitcast.13, bf16[128,2048]{1,0:T(8,128)(2,1)} %refs_4_.1, s32[2,128]{1,0:T(2,128)} %bitcast.11, f32[2,128]{1,0:T(2,128)} %bitcast.12, ...), custom_call_target="tpu_custom_call" | custom-call | tf_op jit(solution)/shard_map/layer/pallas_call | solution.py:1034
  82.6 0.0 copy-start
  82.6 1.7 %copy.24 = bf16[64,2048]{1,0:T(8,128)(2,1)} copy(bf16[64,2048]{1,0:T(8,128)(2,1)} %get-tuple-element.4) | data formatting | bytes 524288
  84.4 0.0 copy-done
  84.4 0.8 copy.25
Async XLA Ops:
  82.6 1.7 %copy-start = (bf16[128,2048]{1,0:T(8,128)(2,1)S(1)}, bf16[128,2048]{1,0:T(8,128)(2,1)}, u32[]{:S(2)}) copy-start(bf16[128,2048]{1,0:T(8,128)(2,1)} %get-tuple-element.5) | copy-start | bytes 1572868

commit v5 on v4

--- a/solution.py
+++ b/solution.py
@@ -427,14 +427,12 @@
     for d in range(early, half):
         at = plan[place[("f", d)]]
         if d == half - 1:
-            at += [("kv_arrivals",), ("head", 0)]
-        if d > early:
-            at += [("core_sum", "f", d - 1)]
+            at += [("core_sum", "f", d - 1), ("kv_arrivals",), ("head", 0)]
         at += [("crossed", "f", d)]
     last = plan[2 * half]
-    last += [("core_sum", "f", half - 1), ("side_sum", early), ("head", 1), ("project_out",)]
-    last += [("side_sum", d) for d in range(early + 1, half)] + [("mix_sum",)]
-    last += [("other_rows", 0), ("other_rows", 1), ("own_rows",)]
+    last += [("core_sum", "f", half - 1), ("side_sum", early), ("other_rows", 0), ("head", 1)]
+    last += [("project_out",)] + [("side_sum", d) for d in range(early + 1, half)]
+    last += [("mix_sum",), ("other_rows", 1), ("own_rows",)]
     return plan
 
 

time: 86.8 us -> 84.1 us (0.969)
  Pallas kernels: 82 us -> 80.1 us
    pallas_call x1, Pallas kernels: 82 us -> 80.1 us  [fused(): pl.pallas_call(functools.partial(fused_kernel, sizes, keys), out_shape=(j...]
where the time goes in v5:
time: 84.1 us; the launch traced here: 83.3 us
  Pallas kernels  80.1 us (95%)
  local copies, waits for them, and re-layouts  2.52 us (3%)
    pallas_call x1, Pallas kernels, fused(): pl.pallas_call(functools.partial(fused_kernel, sizes, keys), out_shape=(j...  80.1 us
    unnamed x4, local copies, waits for them, and re-layouts  2.52 us

profile of v5, /device:TPU:31, one launch (start us, length us, event | category | flops | bytes accessed | tf_op | source)
XLA Modules:
  0.0 83.3 jit_solution(8021256714868898933)
XLA Ops:
  0.6 80.1 %layer.1 = (bf16[64,2048]{1,0:T(8,128)(2,1)}, bf16[128,2048]{1,0:T(8,128)(2,1)}) custom-call(f32[2]{0:T(128)} %refs_0_.1, f32[1,2048]{1,0:T(1,128)} %bitcast.9, f32[1,2048]{1,0:T(1,128)} %bitcast.10, f32[1,128]{1,0:T(1,128)} %bitcast.13, bf16[128,2048]{1,0:T(8,128)(2,1)} %refs_4_.1, s32[2,128]{1,0:T(2,128)} %bitcast.11, f32[2,128]{1,0:T(2,128)} %bitcast.12, ...), custom_call_target="tpu_custom_call" | custom-call | tf_op jit(solution)/shard_map/layer/pallas_call | solution.py:1032
  80.8 0.0 copy-start
  80.8 1.7 %copy.24 = bf16[64,2048]{1,0:T(8,128)(2,1)} copy(bf16[64,2048]{1,0:T(8,128)(2,1)} %get-tuple-element.4) | data formatting | bytes 524288
  82.5 0.0 copy-done
  82.5 0.8 copy.25
Async XLA Ops:
  80.8 1.7 %copy-start = (bf16[128,2048]{1,0:T(8,128)(2,1)S(1)}, bf16[128,2048]{1,0:T(8,128)(2,1)}, u32[]{:S(2)}) copy-start(bf16[128,2048]{1,0:T(8,128)(2,1)} %get-tuple-element.5) | copy-start | bytes 1572868

commit v6 on v5

--- a/solution.py
+++ b/solution.py
@@ -409,9 +409,10 @@
     place = {name: number for number, name in enumerate(order)}
     plan = {number: [] for number in range(2 * half + 1)}
     early = half // 2
+    plan[early] += [("relay_kv",)]
     for d in range(early):
         plan[place[("f", d)]] += [("crossed", "f", d)]
-    plan[early] += [("core_sum", "n", 0), ("relay_kv",)]
+    plan[early] += [("core_sum", "n", 0)]
     first = place[("n", 1)]
     plan[first] += [("crossed", "n", 2)] * (half > 2) + [("arrive_near",)]
     for d in range(3, half):

time: 84.1 us -> 83.5 us (level)
    pallas_call x1, Pallas kernels: 80.1 us -> 79.3 us  [fused(): pl.pallas_call(functools.partial(fused_kernel, sizes, keys), out_shape=(j...]
where the time goes in v6:
time: 83.5 us; the launch traced here: 82.5 us
  Pallas kernels  79.3 us (95%)
  local copies, waits for them, and re-layouts  2.52 us (3%)
    pallas_call x1, Pallas kernels, fused(): pl.pallas_call(functools.partial(fused_kernel, sizes, keys), out_shape=(j...  79.3 us
    unnamed x4, local copies, waits for them, and re-layouts  2.52 us

profile of v6, /device:TPU:31, one launch (start us, length us, event | category | flops | bytes accessed | tf_op | source)
XLA Modules:
  0.0 82.5 jit_solution(2382680713430170730)
XLA Ops:
  0.6 79.3 %layer.1 = (bf16[64,2048]{1,0:T(8,128)(2,1)}, bf16[128,2048]{1,0:T(8,128)(2,1)}) custom-call(f32[2]{0:T(128)} %refs_0_.1, f32[1,2048]{1,0:T(1,128)} %bitcast.9, f32[1,2048]{1,0:T(1,128)} %bitcast.10, f32[1,128]{1,0:T(1,128)} %bitcast.13, bf16[128,2048]{1,0:T(8,128)(2,1)} %refs_4_.1, s32[2,128]{1,0:T(2,128)} %bitcast.11, f32[2,128]{1,0:T(2,128)} %bitcast.12, ...), custom_call_target="tpu_custom_call" | custom-call | tf_op jit(solution)/shard_map/layer/pallas_call | solution.py:1033
  79.9 0.0 copy-start
  79.9 1.7 %copy.24 = bf16[64,2048]{1,0:T(8,128)(2,1)} copy(bf16[64,2048]{1,0:T(8,128)(2,1)} %get-tuple-element.4) | data formatting | bytes 524288
  81.7 0.0 copy-done
  81.7 0.8 copy.25
Async XLA Ops:
  79.9 1.7 %copy-start = (bf16[128,2048]{1,0:T(8,128)(2,1)S(1)}, bf16[128,2048]{1,0:T(8,128)(2,1)}, u32[]{:S(2)}) copy-start(bf16[128,2048]{1,0:T(8,128)(2,1)} %get-tuple-element.5) | copy-start | bytes 1572868
